TPU v7x, 32 devices: a whole 2x2x4 slice. The times are simulated.
32 devices in a mesh: sp: 8 (over z, y), tp: 4 (over x, core).
Axes of the slice: x: 2, y: 2, z: 4, core: 2. Of those that a mesh axis runs over, the one named last changes fastest.
Arguments:
- queries: bfloat16 [6144, 1024], P('sp', 'tp'), may hold values from -8 to 8
- keys: bfloat16 [6144, 256], P('sp', 'tp'), may hold values from -8 to 8
- values: bfloat16 [6144, 256], P('sp', 'tp'), may hold values from -18 to 18
- query_gain: float32 [64], replicated, may hold values from 0.4 to 5.5
- key_gain: float32 [64], replicated, may hold values from 0.4 to 5.5
- sink_logits: float32 [16], P('tp'), may hold values from 2 to 5
- out_weight: bfloat16 [1024, 2048], P('tp'), may hold values from -0.1875 to 0.1875
- residual: bfloat16 [6144, 2048], P('sp', 'tp'), may hold values from -21 to 21
- norm_gain: float32 [2048], P('tp'), may hold values from 0.1 to 1.9
- gate_weight: bfloat16 [2048, 5632], P('sp', 'tp'), may hold values from -0.125 to 0.125
- up_weight: bfloat16 [2048, 5632], P('sp', 'tp'), may hold values from -0.125 to 0.125
- down_weight: bfloat16 [5632, 2048], P('tp', 'sp'), may hold values from -0.078125 to 0.078125
Outputs:
- layer_out: bfloat16 [6144, 2048], P('sp', 'tp')
All inputs are finite; a program needn't handle non-finite values.
Results may differ from a plain program's by a relative error of at most 0.0095.
The roundings to bfloat16 on the way count: a program that leaves them out, or rounds other values in their place, can miss the bound.
Values may be sent and summed in bfloat16 or wider, within the bound.
No kernel may reach another device: no remote copies, remote signals or barrier semaphores. Data moves between devices by JAX's collectives and lax.ppermute only.
A program may use at most 192 MiB of HBM per device.

v0:
```python
import functools

import jax
import jax.numpy as jnp
from jax import lax
from jax.experimental import pallas as pl
from jax.experimental.pallas import tpu as pltpu
from jax.sharding import Mesh
from jax.sharding import PartitionSpec as P


WINDOW = 128
EPS = 1e-06
LANES = 128
MIB = 2**20


def from_behind(block, axes, count):
    return lax.ppermute(block, axes, [(i - 1, i) for i in range(1, count)])


def norm_heads(flat, gain, heads):
    row_count = flat.shape[0]
    head_width = gain.shape[0]
    data = flat.astype(jnp.float32).reshape(row_count, heads, head_width)
    scaled = data * lax.rsqrt(jnp.mean(data * data, axis=-1, keepdims=True) + EPS) * gain
    return scaled.astype(jnp.bfloat16)


def attention(queries, keys, values, query_gain, key_gain, sink_logits, sp_axes, sp_count):
    head_width = query_gain.shape[0]
    row_count = queries.shape[0]
    q_heads = queries.shape[1] // head_width
    k_heads = keys.shape[1] // head_width
    group_size = q_heads // k_heads
    window_len = WINDOW
    block_count = row_count // window_len
    kv_width = k_heads * head_width
    query_norm = norm_heads(queries, query_gain, q_heads)
    key_norm = norm_heads(keys, key_gain, k_heads).reshape(row_count, kv_width)
    tail = jnp.concatenate(
        [key_norm[row_count - window_len :], values[row_count - window_len :]], axis=1
    )
    prev = from_behind(tail, sp_axes, sp_count)
    prev_keys, prev_values = prev[:, :kv_width], prev[:, kv_width:]
    key_all = jnp.concatenate([prev_keys, key_norm], axis=0)
    value_all = jnp.concatenate([prev_values, values], axis=0)

    def blocks(whole, own):
        return jnp.concatenate(
            [
                whole[:row_count].reshape(block_count, window_len, k_heads, head_width),
                own.reshape(block_count, window_len, k_heads, head_width),
            ],
            axis=1,
        )

    key_blocks = blocks(key_all, key_norm)
    value_blocks = blocks(value_all, values)
    query_blocks = query_norm.reshape(block_count, window_len, k_heads, group_size, head_width)
    scores = jnp.einsum(
        "nqhgd,nkhd->nhgqk", query_blocks, key_blocks, preferred_element_type=jnp.float32
    ) * head_width ** (-0.5)
    query_index = jnp.arange(window_len)[:, None]
    key_index = jnp.arange(2 * window_len)[None, :]
    offset_lag = window_len + query_index - key_index
    inband = (offset_lag >= 0) & (offset_lag < window_len)
    leading = (
        (jnp.arange(block_count)[:, None, None] > 0)
        | (key_index[None] >= window_len)
        | (lax.axis_index(sp_axes) > 0)
    )
    valid = inband[None] & leading
    scores = jnp.where(valid[:, None, None], scores, -1e30)
    sink_rows = sink_logits.reshape(k_heads, group_size)[None, :, :, None]
    row_peak = jnp.maximum(jnp.max(scores, axis=-1), sink_rows)
    exp_terms = jnp.exp(scores - row_peak[..., None])
    denom_sum = jnp.sum(exp_terms, axis=-1) + jnp.exp(sink_rows - row_peak)
    weights = (exp_terms / denom_sum[..., None]).astype(jnp.bfloat16)
    attended = jnp.einsum(
        "nhgqk,nkhd->nqhgd", weights, value_blocks, preferred_element_type=jnp.float32
    ).astype(jnp.bfloat16)
    return attended.reshape(row_count, q_heads * head_width)


def general_device(model_width, *args):
    (queries, keys, values, query_gain, key_gain, sink_logits, out_weight, residual) = args[:8]
    (norm_gain, gate_weight, up_weight, down_weight) = args[8:]
    gate_full = lax.all_gather(gate_weight, "sp", axis=0, tiled=True)
    up_full = lax.all_gather(up_weight, "sp", axis=0, tiled=True)
    down_full = lax.all_gather(down_weight, "sp", axis=1, tiled=True)
    attended = attention(
        queries, keys, values, query_gain, key_gain, sink_logits, "sp", lax.axis_size("sp")
    )
    projected = jnp.dot(attended, out_weight, preferred_element_type=jnp.float32)
    mixed = lax.psum_scatter(
        projected.astype(jnp.bfloat16), "tp", scatter_dimension=1, tiled=True
    ).astype(jnp.float32)
    middle_wide = (residual.astype(jnp.float32) + mixed).astype(jnp.bfloat16).astype(jnp.float32)
    squares = lax.psum(jnp.sum(middle_wide * middle_wide, axis=1), "tp")
    scale = lax.rsqrt(squares / model_width + EPS)[:, None]
    normed = (middle_wide * scale * norm_gain).astype(jnp.bfloat16)
    normed_all = lax.all_gather(normed, "tp", axis=1, tiled=True)
    gate_acts = jnp.dot(normed_all, gate_full, preferred_element_type=jnp.float32)
    up_acts = jnp.dot(normed_all, up_full, preferred_element_type=jnp.float32)
    hidden = (jax.nn.silu(gate_acts) * up_acts).astype(jnp.bfloat16)
    down_terms = jnp.dot(hidden, down_full, preferred_element_type=jnp.float32)
    summed_back = lax.psum_scatter(
        down_terms.astype(jnp.bfloat16), "tp", scatter_dimension=1, tiled=True
    ).astype(jnp.float32)
    return (middle_wide + 0.5 * summed_back).astype(jnp.bfloat16)


def swap(block, axis):
    return lax.ppermute(block, axis, [(0, 1), (1, 0)])


def scaled_rows(data, gain):
    wide = data.astype(jnp.float32)
    scale = lax.rsqrt(jnp.mean(wide * wide, axis=-1, keepdims=True) + EPS)
    return (wide * scale * gain).astype(jnp.bfloat16)


def attend_kernel(
    place_ref, sink_ref, q_ref, k_ref, v_ref, halo_ref, qg_ref, kg_ref, out_ref, keys, vals
):
    step = pl.program_id(0)
    width, window = k_ref.shape[0], q_ref.shape[0]
    heads = q_ref.shape[1] // width

    @pl.when(step == 0)
    def _():
        def scaled_columns(data):
            wide = data.astype(jnp.float32)
            scale = lax.rsqrt(jnp.mean(wide * wide, axis=0, keepdims=True) + EPS)
            return (wide * scale * kg_ref[...]).astype(jnp.bfloat16)

        keys[:, :window] = scaled_columns(halo_ref[:width, :])
        keys[:, window:] = scaled_columns(k_ref[...])
        vals[:, :window] = halo_ref[width:, :]
        vals[:, window:] = v_ref[...]

    span = pl.ds(pl.multiple_of(step * window, window), 2 * window)
    part = [scaled_rows(q_ref[:, h * width : (h + 1) * width], qg_ref[...]) for h in range(heads)]
    scores = jnp.dot(
        jnp.concatenate(part, axis=0), keys[:, span], preferred_element_type=jnp.float32
    ) * width ** (-0.5)
    shape = (window, 2 * window)
    column = lax.broadcasted_iota(jnp.int32, shape, 1)
    lag = window + lax.broadcasted_iota(jnp.int32, shape, 0) - column
    starts = (step > 0) | (place_ref[0] > 0)
    valid = (lag >= 0) & (lag < window) & ((column >= window) | starts)
    weights = []
    for h in range(heads):
        sink = sink_ref[h]
        score = jnp.where(valid, scores[h * window : (h + 1) * window], -1e30)
        peak = jnp.maximum(jnp.max(score, axis=-1, keepdims=True), sink)
        terms = jnp.exp(score - peak)
        total = jnp.sum(terms, axis=-1, keepdims=True) + jnp.exp(sink - peak)
        weights.append((terms / total).astype(jnp.bfloat16))
    mixed = lax.dot_general(
        jnp.concatenate(weights, axis=0),
        vals[:, span],
        (((1,), (1,)), ((), ())),
        preferred_element_type=jnp.float32,
    ).astype(jnp.bfloat16)
    out_ref[...] = jnp.concatenate(
        [mixed[h * window : (h + 1) * window] for h in range(heads)], axis=1
    )


def attend(place, sinks, queries, keys, values, halo, query_gain, key_gain):
    width, rows = keys.shape
    window = WINDOW
    full = lambda a: pl.BlockSpec(a.shape, lambda i, p, s: (0,) * a.ndim)
    row_spec = pl.BlockSpec((window, queries.shape[1]), lambda i, p, s: (i, 0))
    gains = (query_gain[None], key_gain[:, None])
    return pl.pallas_call(
        attend_kernel,
        grid_spec=pltpu.PrefetchScalarGridSpec(
            num_scalar_prefetch=2,
            grid=(rows // window,),
            in_specs=[row_spec, full(keys), full(values), full(halo), *map(full, gains)],
            out_specs=row_spec,
            scratch_shapes=[pltpu.VMEM((width, rows + window), jnp.bfloat16)] * 2,
        ),
        out_shape=jax.ShapeDtypeStruct(queries.shape, jnp.bfloat16),
        cost_estimate=pl.CostEstimate(
            flops=rows * window * width * 400, bytes_accessed=rows * 1024, transcendentals=0
        ),
        name="attend",
    )(place, sinks, queries, keys, values, halo, *gains)


def halves_kernel(main, tail, place_ref, gate_ref, up_ref, own_ref, far_ref):
    def put(ref, h):
        ref[:, :main] = gate_ref[:, h * main : (h + 1) * main]
        ref[:, main : 2 * main] = up_ref[:, h * main : (h + 1) * main]
        if tail:
            rest = [r[:, 2 * main :][:, h * tail : (h + 1) * tail] for r in (gate_ref, up_ref)]
            ref[:, 2 * main :] = jnp.concatenate(rest, axis=1)

    for low in (0, 1):

        @pl.when(place_ref[0] == low)
        def _():
            put(own_ref, low)
            put(far_ref, 1 - low)


def down_halves_kernel(main, tail, place_ref, down_ref, own_ref, far_ref):
    def put(ref, h):
        ref[:main, :] = down_ref[h * main : (h + 1) * main, :]
        if tail:
            ref[main:, :] = down_ref[2 * main + h * tail : 2 * main + (h + 1) * tail, :]

    for low in (0, 1):

        @pl.when(place_ref[0] == low)
        def _():
            put(own_ref, low)
            put(far_ref, 1 - low)


def split(kernel, place, shape, *weights):
    spec = lambda s: pl.BlockSpec(s, lambda i, p: (0, 0))
    return pl.pallas_call(
        kernel,
        grid_spec=pltpu.PrefetchScalarGridSpec(
            num_scalar_prefetch=1,
            grid=(1,),
            in_specs=[spec(w.shape) for w in weights],
            out_specs=[spec(shape)] * 2,
        ),
        out_shape=[jax.ShapeDtypeStruct(shape, jnp.bfloat16)] * 2,
        cost_estimate=pl.CostEstimate(flops=10**9, bytes_accessed=10**6, transcendentals=0),
    )(place, *weights)


def project_kernel(place_ref, *refs):
    atts, outs, ress, gains = (refs[4 * n : 4 * n + 4] for n in range(4))
    normed_ref, middle_ref, held = refs[16:]
    width = ress[0].shape[1]
    columns = [pl.ds(pl.multiple_of(place_ref[n] * width, width), width) for n in range(4)]
    squares = 0.0
    for n in range(4):
        total = sum(
            jnp.dot(a[...], o[:, columns[n]], preferred_element_type=jnp.float32)
            for a, o in zip(atts, outs)
        )
        middle = (total + ress[n][...].astype(jnp.float32)).astype(jnp.bfloat16)
        wide = middle.astype(jnp.float32)
        squares += jnp.sum(wide * wide, axis=1, keepdims=True)
        held[n] = middle
    scale = lax.rsqrt(squares / (4 * width) + EPS)
    for n in range(4):
        wide = held[n].astype(jnp.float32)
        normed_ref[:, columns[n]] = (wide * scale * gains[n][...]).astype(jnp.bfloat16)
    middle_ref[...] = held[0]


def project(place, atts, outs, ress, gains, tile):
    rows, depth = atts[0].shape
    width = outs[0].shape[1]
    part = ress[0].shape[1]
    row_spec = lambda n: pl.BlockSpec((tile, n), lambda i, p: (i, 0))
    full_spec = lambda a: pl.BlockSpec(a.shape, lambda i, p: (0, 0))
    return pl.pallas_call(
        project_kernel,
        grid_spec=pltpu.PrefetchScalarGridSpec(
            num_scalar_prefetch=1,
            grid=(rows // tile,),
            in_specs=[row_spec(depth)] * 4
            + [full_spec(o) for o in outs]
            + [row_spec(part)] * 4
            + [full_spec(g) for g in gains],
            out_specs=[row_spec(width), row_spec(part)],
            scratch_shapes=[pltpu.VMEM((4, tile, part), jnp.bfloat16)],
        ),
        out_shape=[
            jax.ShapeDtypeStruct((rows, width), jnp.bfloat16),
            jax.ShapeDtypeStruct((rows, part), jnp.bfloat16),
        ],
        compiler_params=pltpu.CompilerParams(vmem_limit_bytes=60 * MIB),
        cost_estimate=pl.CostEstimate(
            flops=8 * rows * depth * width, bytes_accessed=4 * rows * width, transcendentals=0
        ),
    )(place, *atts, *outs, *ress, *gains)


def partial_kernel(count, place_ref, x_ref, *refs):
    pieces, out_ref, whole = refs[:count], refs[count], refs[count + 1]
    depth = pieces[0].shape[0]

    @pl.when(pl.program_id(0) == 0)
    def _():
        for n, piece in enumerate(pieces):
            whole[n * depth : (n + 1) * depth, :] = piece[...]

    columns = [pl.ds(pl.multiple_of(place_ref[n] * depth, depth), depth) for n in range(count)]
    x = jnp.concatenate([x_ref[:, c] for c in columns], axis=1)
    out_ref[...] = jnp.dot(x, whole[...], preferred_element_type=jnp.float32)


def partial_acts(place, x, pieces, tile):
    rows, depth = x.shape
    count, (piece, width) = len(pieces), pieces[0].shape
    return pl.pallas_call(
        functools.partial(partial_kernel, count),
        grid_spec=pltpu.PrefetchScalarGridSpec(
            num_scalar_prefetch=1,
            grid=(rows // tile,),
            in_specs=[pl.BlockSpec((tile, depth), lambda i, p: (i, 0))]
            + [pl.BlockSpec(p.shape, lambda i, p: (0, 0)) for p in pieces],
            out_specs=pl.BlockSpec((tile, width), lambda i, p: (i, 0)),
            scratch_shapes=[pltpu.VMEM((count * piece, width), jnp.bfloat16)],
        ),
        out_shape=jax.ShapeDtypeStruct((rows, width), jnp.float32),
        compiler_params=pltpu.CompilerParams(vmem_limit_bytes=60 * MIB),
        cost_estimate=pl.CostEstimate(
            flops=2 * rows * count * piece * width, bytes_accessed=4 * rows * width,
            transcendentals=0,
        ),
    )(place, x, *pieces)


def hidden_kernel(main, tail, early, count, place_ref, near_ref, far_ref, acts_ref, *refs):
    pieces, out_ref, whole = refs[:count], refs[count], refs[count + 1]
    depth = near_ref.shape[1] // 8
    step = pl.program_id(0)
    middle = pl.num_programs(0) // 2

    @pl.when(step == 0)
    def _():
        start = 0
        for piece in pieces:
            whole[start : start + piece.shape[0], :] = piece[...]
            start += piece.shape[0]

    def gated(gate, up):
        return (gate / (1.0 + jnp.exp(-gate)) * up).astype(jnp.bfloat16)

    def product(x_ref, first):
        columns = [
            pl.ds(pl.multiple_of(place_ref[n] * depth, depth), depth) for n in range(first, 8)
        ]
        x = jnp.concatenate([x_ref[:, c] for c in columns], axis=1)
        return jnp.dot(x, whole[first * depth :, :], preferred_element_type=jnp.float32)

    def finish(acts):
        out_ref[:, :main] = gated(acts[:, :main], acts[:, main : 2 * main])
        if tail:
            rest = acts[:, 2 * main :]
            out_ref[:, main:] = gated(rest[:, :tail], rest[:, tail:])

    pl.when(step < middle)(lambda: finish(acts_ref[...] + product(near_ref, early)))
    pl.when(step >= middle)(lambda: finish(product(far_ref, 0)))


def hidden_units(place, near, far, acts, pieces, early, main, tail, tile):
    rows, depth = near.shape
    width = pieces[0].shape[1]
    tiles = rows // tile
    first = lambda i, p: (jnp.minimum(i, tiles - 1), 0)
    second = lambda i, p: (jnp.maximum(i - tiles, 0), 0)
    return pl.pallas_call(
        functools.partial(hidden_kernel, main, tail, early, len(pieces)),
        grid_spec=pltpu.PrefetchScalarGridSpec(
            num_scalar_prefetch=1,
            grid=(2 * tiles,),
            in_specs=[
                pl.BlockSpec((tile, depth), first),
                pl.BlockSpec((tile, depth), second),
                pl.BlockSpec((tile, width), first),
            ]
            + [pl.BlockSpec(p.shape, lambda i, p: (0, 0)) for p in pieces],
            out_specs=pl.BlockSpec((tile, main + tail), lambda i, p: (i, 0)),
            scratch_shapes=[pltpu.VMEM((depth, width), jnp.bfloat16)],
        ),
        out_shape=jax.ShapeDtypeStruct((2 * rows, main + tail), jnp.bfloat16),
        compiler_params=pltpu.CompilerParams(vmem_limit_bytes=40 * MIB),
        cost_estimate=pl.CostEstimate(
            flops=3 * rows * depth * width, bytes_accessed=8 * rows * width, transcendentals=0
        ),
        name="hidden_units",
    )(place, near, far, acts, *pieces)


def down_kernel(kept, flag_ref, hidden_ref, *refs):
    pieces, (*got_ref, out_ref, whole) = refs[:4], refs[4:]
    block = pieces[0].shape[1]

    @pl.when(pl.program_id(0) == 0)
    def _():
        for same in (0, 1):
            for near in (0, 1):

                @pl.when((flag_ref[0] == same) & (flag_ref[1] == near))
                def _():
                    for n, piece in enumerate(pieces):
                        if ((n % 2) != same) == kept:
                            at = block if (n // 2) == near else 0
                            whole[:, at : at + block] = piece[...]

    acts = jnp.dot(hidden_ref[...], whole[...], preferred_element_type=jnp.float32)
    if kept:
        acts += got_ref[0][...].astype(jnp.float32)
    out_ref[...] = acts.astype(jnp.bfloat16)


def down(flags, hidden, pieces, tile, got=()):
    rows, depth = hidden.shape
    block = pieces[0].shape[1]
    row_spec = lambda n: pl.BlockSpec((tile, n), lambda i, p: (i, 0))
    return pl.pallas_call(
        functools.partial(down_kernel, bool(got)),
        grid_spec=pltpu.PrefetchScalarGridSpec(
            num_scalar_prefetch=1,
            grid=(rows // tile,),
            in_specs=[row_spec(depth)]
            + [pl.BlockSpec(p.shape, lambda i, p: (0, 0)) for p in pieces]
            + [row_spec(2 * block)] * len(got),
            out_specs=row_spec(2 * block),
            scratch_shapes=[pltpu.VMEM((depth, 2 * block), jnp.bfloat16)],
        ),
        out_shape=jax.ShapeDtypeStruct((rows, 2 * block), jnp.bfloat16),
        compiler_params=pltpu.CompilerParams(vmem_limit_bytes=20 * MIB),
        cost_estimate=pl.CostEstimate(
            flops=4 * rows * depth * block, bytes_accessed=4 * rows * block, transcendentals=0
        ),
    )(flags, hidden, *pieces, *got)


def finish_kernel(flag_ref, middle_ref, ahead_ref, ahead_got, behind_ref, behind_got, out_ref):
    block = ahead_ref.shape[1]
    pairs = ((ahead_ref, ahead_got), (behind_ref, behind_got))
    for odd in (0, 1):

        @pl.when(flag_ref[0] == odd)
        def _():
            for n, (kept, got) in enumerate(pairs):
                columns = slice((n ^ odd) * block, ((n ^ odd) + 1) * block)
                feed = kept[...].astype(jnp.float32) + got[...].astype(jnp.float32)
                total = middle_ref[:, columns].astype(jnp.float32) + 0.5 * feed
                out_ref[:, columns] = total.astype(jnp.bfloat16)


def finish(flag, middle, ahead, ahead_got, behind, behind_got):
    rows, width = middle.shape
    block = ahead.shape[1]
    tile = rows // 2
    wide = pl.BlockSpec((tile, width), lambda i, p: (i, 0))
    half = pl.BlockSpec((tile, block), lambda i, p: (i, 0))
    return pl.pallas_call(
        finish_kernel,
        grid_spec=pltpu.PrefetchScalarGridSpec(
            num_scalar_prefetch=1,
            grid=(2,),
            in_specs=[wide, half, half, half, half],
            out_specs=wide,
        ),
        out_shape=jax.ShapeDtypeStruct((rows, width), jnp.bfloat16),
        cost_estimate=pl.CostEstimate(
            flops=rows * width * 8, bytes_accessed=rows * width * 8, transcendentals=0
        ),
        name="finish",
    )(flag, middle, ahead, ahead_got, behind, behind_got)


def paired_device(
    queries, keys, values, query_gain, key_gain, sink_logits, out_weight, residual, norm_gain,
    gate_weight, up_weight, down_weight,
):
    zh, zl, y, x, c = (lax.axis_index(a) for a in ("zh", "zl", "y", "x", "c"))
    rows = queries.shape[0]
    block = down_weight.shape[1]
    units = gate_weight.shape[1]
    main = units // LANES // 2 * LANES
    tail = (units - 2 * main) // 2
    one = lambda v: v.astype(jnp.int32).reshape(1)

    sp_axes = ("zh", "zl", "y")
    keys, values = keys.T, values.T
    edge = jnp.concatenate([keys[:, rows - WINDOW :], values[:, rows - WINDOW :]], axis=0)
    halo = from_behind(edge, sp_axes, lax.axis_size(sp_axes))

    gu_own, gu_far = split(
        functools.partial(halves_kernel, main, tail), one(zl),
        gate_weight.shape, gate_weight, up_weight,
    )
    gu_swp = swap(gu_far, "zl")
    gu_own_m = swap(gu_own, "zh")
    gu_own_y = swap(gu_own, "y")
    res2 = swap(residual, "zl")
    dn_own, dn_far = split(
        functools.partial(down_halves_kernel, main, tail), one(zl),
        (main + tail, block), down_weight,
    )
    attended = attend(
        one(lax.axis_index(sp_axes)), sink_logits, queries, keys, values, halo, query_gain,
        key_gain,
    )
    att2 = swap(attended, "zl")
    part = gu_swp.shape[0] // 2
    gu_swp_m = [swap(gu_swp[n * part : (n + 1) * part], "zh") for n in (0, 1)]
    gu_swp_y = swap(gu_swp, "y")
    dn_swp = swap(dn_far, "zl")
    dn_own_m = swap(dn_own, "zh")
    dn_own_y = swap(dn_own, "y")
    gu_own_my = swap(gu_own_m, "y")

    place = jnp.stack(
        [2 * x + c, 2 * (1 - x) + c, 2 * x + (1 - c), 2 * (1 - x) + (1 - c)]
    ).astype(jnp.int32)

    def over_tp(own):
        far = swap(own, "x")
        return own, far, swap(own, "c"), swap(far, "c")

    gains = over_tp(norm_gain[None])
    outs = over_tp(out_weight)
    normed, middle = project(
        place, over_tp(attended), outs, over_tp(residual), gains,
        256,
    )
    normed2, _ = project(place, over_tp(att2), outs, over_tp(res2), gains, 256)

    gu_swp_my = [swap(gu_swp_m[n], "y") for n in (0, 1)]
    dn_swp_m = swap(dn_swp, "zh")
    dn_swp_y = swap(dn_swp, "y")
    dn_own_my = swap(dn_own_m, "y")
    dn_swp_my = swap(dn_swp_m, "y")

    pieces = [gu_own, gu_own_y, gu_swp, gu_swp_y, gu_own_m, gu_own_my]
    at = lambda n: 4 * (zh ^ (n // 4)) + 2 * (zl ^ (n // 2 % 2)) + (y ^ (n % 2))
    spots = jnp.stack([at(n) for n in range(8)]).astype(jnp.int32)
    acts = partial_acts(spots[:6], normed, pieces, rows // 2)
    hidden = hidden_units(
        spots, normed, normed2, acts, [*pieces, *gu_swp_m, *gu_swp_my], 6, main, tail, rows // 2
    )

    flags = jnp.stack([c == zl, x == zh]).astype(jnp.int32)
    wide = lambda v: v.astype(jnp.float32)
    add = lambda a, b: wide(a) + wide(b)

    def reduced(pieces, rows_first):
        sent = down(flags, hidden, pieces, rows // 2)
        got = swap(sent, "c")
        total = down(flags, hidden, pieces, rows // 2, (got,))
        if rows_first:
            got = swap(total[rows:], "zl")
            total = add(total[:rows], got).astype(jnp.bfloat16)
            return total[:, :block], swap(total[:, block:], "x")
        got = swap(total[:, block:], "x")
        total = add(total[:, :block], got).astype(jnp.bfloat16)
        return total[:rows], swap(total[rows:], "zl")

    ahead = reduced((dn_own, dn_swp, dn_own_m, dn_swp_m), True)
    behind = reduced((dn_own_y, dn_swp_y, dn_own_my, dn_swp_my), False)
    return finish(one(y), middle, *ahead, *behind)


def solution(mesh):
    sp, tp = mesh.shape["sp"], mesh.shape["tp"]

    def spread(fine, sp_axes, tp_axes, body):
        both = P(sp_axes, tp_axes)
        heads, rows = P(tp_axes), P(tp_axes, None)
        in_specs = (both, both, both, P(), P(), heads, rows, both, heads, both, both)
        return jax.shard_map(
            body,
            mesh=fine,
            in_specs=(*in_specs, P(tp_axes, sp_axes)),
            out_specs=both,
            check_vma=False,
        )

    def step(*args):
        if (sp, tp) == (8, 4) and args[1].shape[1] == tp * args[3].shape[0]:
            fine = Mesh(mesh.devices.reshape(2, 2, 2, 2, 2), ("zh", "zl", "y", "x", "c"))
            return spread(fine, ("zh", "zl", "y"), ("x", "c"), paired_device)(*args)
        body = functools.partial(general_device, args[8].shape[0])
        return spread(mesh, "sp", "tp", body)(*args)

    return step
```

profile of v0, /device:TPU:0, one launch (start us, length us, event | category | flops | bytes accessed | tf_op | source)
XLA Modules:
  0.0 282.2 jit_solution(4153924399204784863)
XLA Ops:
  1.4 4.9 %collective-permute-start = (bf16[128,128]{1,0:T(8,128)(2,1)S(1)}, bf16[128,128]{1,0:T(8,128)(2,1)S(1)}, u32[]{:S(2)}, u32[]{:S(2)}) collective-permute-start(bf16[128,128]{1,0:T(8,128)(2,1)S(1)} %pad_maximum_fusion), channel_id=1, source_target_pairs={{0,4},{4,8},{8,12},{12,16},{16,20},{20,24},{24,28},{1,5},{5,9},{9,... | collective-permute-start | bytes 98312 | tf_op jit(solution)/shard_map/ppermute | solution.py:19
  6.3 2.6 shard_map.120
  8.9 1.5 collective-permute-start.21
  10.4 2.0 shard_map.122
  12.5 1.6 collective-permute-start.30
  15.4 8.3 %attend.1.refs_0_ = bf16[768,256]{1,0:T(8,128)(2,1)} custom-call(s32[1]{0:T(128)} %bitcast.5.place_ref, f32[4]{0:T(128)} %sink_ref.1, bf16[768,256]{1,0:T(8,128)(2,1)} %q_ref.1, bf16[64,768]{1,0:T(8,128)(2,1)} %bitcast.23, bf16[64,768]{1,0:T(8,128)(2,1)} %bitcast.25, bf16[128,128]{1,0:T(8,128)(2,1)} %copy-done.23, f32[1,64]{1,0:T(1,128)} %bitcast.31, ...), custom_call_target="tpu_custom_call" | custom-call | flops 2516582400 | bytes 786432 | tf_op jit(solution)/shard_map/attend/pallas_call | solution.py:178
  23.7 1.5 collective-permute-start.1
  25.7 8.2 %collective-permute-done.10.refs_13_ = f32[1,512]{1,0:T(1,128)S(1)} collective-permute-done((f32[1,512]{1,0:T(1,128)S(1)}, f32[1,512]{1,0:T(1,128)S(1)}, u32[]{:S(2)}, u32[]{:S(2)}) %collective-permute-start.10) | collective-permute-done | bytes 2080 | tf_op jit(solution)/shard_map/ppermute | solution.py:115
  35.6 1.6 collective-permute-start.22
  37.1 1.4 collective-permute-start.24
  38.6 1.5 collective-permute-start.7
  40.1 22.7 %collective-permute-done.13.refs_0_ = bf16[768,256]{1,0:T(8,128)(2,1)S(1)} collective-permute-done((bf16[768,256]{1,0:T(8,128)(2,1)}, bf16[768,256]{1,0:T(8,128)(2,1)S(1)}, u32[]{:S(2)}, u32[]{:S(2)}) %collective-permute-start.13) | collective-permute-done | bytes 393248 | tf_op jit(solution)/shard_map/ppermute | solution.py:115
  62.8 1.6 collective-permute-start.4
  64.3 13.1 %collective-permute-done.22.refs_2_ = bf16[256,1408]{1,0:T(8,128)(2,1)S(1)} collective-permute-done((bf16[256,1408]{1,0:T(8,128)(2,1)}, bf16[256,1408]{1,0:T(8,128)(2,1)S(1)}, u32[]{:S(2)}, u32[]{:S(2)}) %collective-permute-start.22) | collective-permute-done | bytes 720928 | tf_op jit(solution)/shard_map/ppermute | solution.py:115
  78.0 1.5 collective-permute-start.14
  79.5 17.1 %collective-permute-done.17.refs_8_ = bf16[768,512]{1,0:T(8,128)(2,1)} collective-permute-done((bf16[768,512]{1,0:T(8,128)(2,1)}, bf16[768,512]{1,0:T(8,128)(2,1)}, u32[]{:S(2)}, u32[]{:S(2)}) %collective-permute-start.17) | collective-permute-done | bytes 786464 | tf_op jit(solution)/shard_map/ppermute | solution.py:115
  97.1 1.5 collective-permute-start.18
  98.8 1.4 collective-permute-start.26
  100.1 1.6 collective-permute-start.27
  101.8 24.2 %collective-permute-done.26.refs_6_ = bf16[128,1408]{1,0:T(8,128)(2,1)} collective-permute-done((bf16[128,1408]{1,0:T(8,128)(2,1)S(1)}, bf16[128,1408]{1,0:T(8,128)(2,1)}, u32[]{:S(2)}, u32[]{:S(2)}) %collective-permute-start.26) | collective-permute-done | bytes 360480 | tf_op jit(solution)/shard_map/ppermute | solution.py:115
  126.5 7.2 %collective-permute-done.27.refs_7_ = bf16[128,1408]{1,0:T(8,128)(2,1)} collective-permute-done((bf16[128,1408]{1,0:T(8,128)(2,1)S(1)}, bf16[128,1408]{1,0:T(8,128)(2,1)}, u32[]{:S(2)}, u32[]{:S(2)}) %collective-permute-start.27) | collective-permute-done | bytes 360480 | tf_op jit(solution)/shard_map/ppermute | solution.py:115
  136.3 9.9 %shard_map.118 = (bf16[768,2048]{1,0:T(8,128)(2,1)}, bf16[768,512]{1,0:T(8,128)(2,1)}) custom-call(s32[4]{0:T(128)} %pad_add_fusion.place_ref, bf16[768,256]{1,0:T(8,128)(2,1)} %attend.1.refs_0_, bf16[768,256]{1,0:T(8,128)(2,1)} %copy-done.19, bf16[768,256]{1,0:T(8,128)(2,1)} %copy-done.20, bf16[768,256]{1,0:T(8,128)(2,1)} %copy-done.22, ...), custom_call_target="tpu_custom_call" | custom-call | flops 3221225472 | bytes 6291456 | tf_op jit(solution)/shard_map/pallas_call | solution.py:268
  146.2 1.6 collective-permute-start.28
  147.8 12.7 %collective-permute-done.25.refs_5_ = bf16[256,1408]{1,0:T(8,128)(2,1)} collective-permute-done((bf16[256,1408]{1,0:T(8,128)(2,1)S(1)}, bf16[256,1408]{1,0:T(8,128)(2,1)}, u32[]{:S(2)}, u32[]{:S(2)}) %collective-permute-start.25) | collective-permute-done | bytes 720928 | tf_op jit(solution)/shard_map/ppermute | solution.py:115
  161.0 9.2 %shard_map.121.acts_ref = f32[768,1408]{1,0:T(8,128)} custom-call(s32[6]{0:T(128)} %stack.70.place_ref, bf16[768,2048]{1,0:T(8,128)(2,1)} %get-tuple-element.13.x_ref.near_ref, bf16[256,1408]{1,0:T(8,128)(2,1)} %get-tuple-element.15.refs_0_, bf16[256,1408]{1,0:T(8,128)(2,1)} %copy-done.5, bf16[256,1408]{1,0:T(8,128)(2,1)} %copy-done.1, ...), custom_call_target="tpu_custom_call" | custom-call | flops 3321888768 | bytes 4325376 | tf_op jit(solution)/shard_map/pallas_call | solution.py:308
  170.4 2.9 %collective-permute-start.32 = (bf16[704,256]{1,0:T(8,128)(2,1)S(1)}, bf16[704,256]{1,0:T(8,128)(2,1)S(1)}, u32[]{:S(2)}, u32[]{:S(2)}) collective-permute-start(bf16[704,256]{1,0:T(8,128)(2,1)S(1)} %collective-permute-done.30.refs_1_), channel_id=1, source_target_pairs={{0,16},{16,0},{1,17},{17,1},{2,18},{18,2},{3,19},{19,3},{4,20},{20... | collective-permute-start | bytes 1081352 | tf_op jit(solution)/shard_map/ppermute | solution.py:115
  173.3 9.8 %shard_map.119 = (bf16[768,2048]{1,0:T(8,128)(2,1)}, bf16[768,512]{1,0:T(8,128)(2,1)}) custom-call(s32[4]{0:T(128)} %pad_add_fusion.place_ref, bf16[768,256]{1,0:T(8,128)(2,1)} %copy-done.18, bf16[768,256]{1,0:T(8,128)(2,1)} %collective-permute-done.14.refs_1_, bf16[768,256]{1,0:T(8,128)(2,1)} %copy-done.21, ...), custom_call_target="tpu_custom_call" | custom-call | flops 3221225472 | bytes 6291456 | tf_op jit(solution)/shard_map/pallas_call | solution.py:268
  184.2 1.1 copy-done.10
  185.4 1.9 copy-done.11
  187.2 1.9 copy-done.12
  189.1 10.4 %hidden_units.1.hidden_ref = bf16[1536,704]{1,0:T(8,128)(2,1)S(1)} custom-call(s32[8]{0:T(128)S(1)} %stack.69.place_ref, bf16[768,2048]{1,0:T(8,128)(2,1)S(1)} %copy-done.11, bf16[768,2048]{1,0:T(8,128)(2,1)S(1)} %copy-done.12, f32[768,1408]{1,0:T(8,128)} %shard_map.121.acts_ref, bf16[256,1408]{1,0:T(8,128)(2,1)S(1)} %copy-done.4, ...), custom_call_target="tpu_custom_call" | custom-call | flops 6643777536 | bytes 8650752 | tf_op jit(solution)/shard_map/hidden_units/pallas_call | solution.py:366
  199.6 2.9 %collective-permute-done.32.refs_3_ = bf16[704,256]{1,0:T(8,128)(2,1)S(1)} collective-permute-done((bf16[704,256]{1,0:T(8,128)(2,1)S(1)}, bf16[704,256]{1,0:T(8,128)(2,1)S(1)}, u32[]{:S(2)}, u32[]{:S(2)}) %collective-permute-start.32) | collective-permute-done | bytes 360480 | tf_op jit(solution)/shard_map/ppermute | solution.py:115
  202.4 2.6 shard_map.123
  205.1 1.6 collective-permute-start.36
  207.2 1.5 collective-permute-start.38
  209.2 7.2 %collective-permute-done.36.refs_0_ = bf16[704,256]{1,0:T(8,128)(2,1)S(1)} collective-permute-done((bf16[704,256]{1,0:T(8,128)(2,1)S(1)}, bf16[704,256]{1,0:T(8,128)(2,1)S(1)}, u32[]{:S(2)}, u32[]{:S(2)}) %collective-permute-start.36) | collective-permute-done | bytes 360480 | tf_op jit(solution)/shard_map/ppermute | solution.py:115
  216.4 7.7 %collective-permute-done.37.refs_1_ = bf16[704,256]{1,0:T(8,128)(2,1)S(1)} collective-permute-done((bf16[704,256]{1,0:T(8,128)(2,1)S(1)}, bf16[704,256]{1,0:T(8,128)(2,1)S(1)}, u32[]{:S(2)}, u32[]{:S(2)}) %collective-permute-start.37) | collective-permute-done | bytes 360480 | tf_op jit(solution)/shard_map/ppermute | solution.py:115
  224.2 7.7 %collective-permute-done.38.refs_2_ = bf16[704,256]{1,0:T(8,128)(2,1)S(1)} collective-permute-done((bf16[704,256]{1,0:T(8,128)(2,1)S(1)}, bf16[704,256]{1,0:T(8,128)(2,1)S(1)}, u32[]{:S(2)}, u32[]{:S(2)}) %collective-permute-start.38) | collective-permute-done | bytes 360480 | tf_op jit(solution)/shard_map/ppermute | solution.py:115
  231.9 7.2 %collective-permute-done.39.refs_3_ = bf16[704,256]{1,0:T(8,128)(2,1)S(1)} collective-permute-done((bf16[704,256]{1,0:T(8,128)(2,1)S(1)}, bf16[704,256]{1,0:T(8,128)(2,1)S(1)}, u32[]{:S(2)}, u32[]{:S(2)}) %collective-permute-start.39) | collective-permute-done | bytes 360480 | tf_op jit(solution)/shard_map/ppermute | solution.py:115
  239.1 2.7 shard_map.125
  241.9 2.6 shard_map.124
  245.3 2.6 shard_map.126
  248.4 16.1 %collective-permute-done.34 = bf16[768,512]{1,0:T(8,128)(2,1)S(1)} collective-permute-done((bf16[768,512]{1,0:T(8,128)(2,1)S(1)}, bf16[768,512]{1,0:T(8,128)(2,1)S(1)}, u32[]{:S(2)}, u32[]{:S(2)}) %collective-permute-start.34) | collective-permute-done | bytes 786464 | tf_op jit(solution)/shard_map/ppermute | solution.py:115
  266.0 1.5 collective-permute-done.41
  268.6 2.0 collective-permute-start.42
  270.6 5.6 %collective-permute-done.35.ahead_got = bf16[768,256]{1,0:T(8,128)(2,1)S(1)} collective-permute-done((bf16[768,256]{1,0:T(8,128)(2,1)S(1)}, bf16[768,256]{1,0:T(8,128)(2,1)S(1)}, u32[]{:S(2)}, u32[]{:S(2)}) %collective-permute-start.35) | collective-permute-done | bytes 393248 | tf_op jit(solution)/shard_map/ppermute | solution.py:115
  276.2 2.7 collective-permute-done.42.behind_got
  279.6 2.6 finish.1
  (121 shorter events, 16.8 us)
Async XLA Ops:
  1.4 13.3 %collective-permute-start = (bf16[128,128]{1,0:T(8,128)(2,1)S(1)}, bf16[128,128]{1,0:T(8,128)(2,1)S(1)}, u32[]{:S(2)}, u32[]{:S(2)}) collective-permute-start(bf16[128,128]{1,0:T(8,128)(2,1)S(1)} %pad_maximum_fusion), channel_id=1, source_target_pairs={{0,4},{4,8},{8,12},{12,16},{16,20},{20,24},{24,28},{1,5},{5,9},{9,... | collective-permute-start | bytes 98312 | tf_op jit(solution)/shard_map/ppermute | solution.py:19
  8.9 53.8 %collective-permute-start.21 = (bf16[256,1408]{1,0:T(8,128)(2,1)}, bf16[256,1408]{1,0:T(8,128)(2,1)S(1)}, u32[]{:S(2)}, u32[]{:S(2)}) collective-permute-start(bf16[256,1408]{1,0:T(8,128)(2,1)} %get-tuple-element.15.refs_0_), channel_id=1, source_target_pairs={{0,4},{4,0},{1,5},{5,1},{2,6},{6,2},{3,7},{7,3},{8,12},{12,8},{9,1... | collective-permute-start | bytes 2162696 | tf_op jit(solution)/shard_map/ppermute | solution.py:115
  12.5 23.1 %collective-permute-start.30 = (bf16[704,256]{1,0:T(8,128)(2,1)}, bf16[704,256]{1,0:T(8,128)(2,1)S(1)}, u32[]{:S(2)}, u32[]{:S(2)}) collective-permute-start(bf16[704,256]{1,0:T(8,128)(2,1)} %get-tuple-element.18), channel_id=1, source_target_pairs={{0,8},{8,0},{1,9},{9,1},{2,10},{10,2},{3,11},{11,3},{4,12},{12,4},... | collective-permute-start | bytes 1081352 | tf_op jit(solution)/shard_map/ppermute | solution.py:115
  23.7 13.5 %collective-permute-start.1 = (bf16[768,256]{1,0:T(8,128)(2,1)}, bf16[768,256]{1,0:T(8,128)(2,1)S(1)}, u32[]{:S(2)}, u32[]{:S(2)}) collective-permute-start(bf16[768,256]{1,0:T(8,128)(2,1)} %attend.1.refs_0_), channel_id=1, source_target_pairs={{0,2},{2,0},{1,3},{3,1},{4,6},{6,4},{5,7},{7,5},{8,10},{10,8},{9,1... | collective-permute-start | bytes 1179656 | tf_op jit(solution)/shard_map/ppermute | solution.py:115
  25.1 8.8 %collective-permute-start.10 = (f32[1,512]{1,0:T(1,128)S(1)}, f32[1,512]{1,0:T(1,128)S(1)}, u32[]{:S(2)}, u32[]{:S(2)}) collective-permute-start(f32[1,512]{1,0:T(1,128)S(1)} %bitcast.29), channel_id=1, source_target_pairs={{0,2},{2,0},{1,3},{3,1},{4,6},{6,4},{5,7},{7,5},{8,10},{10,8},{9,1... | collective-permute-start | bytes 6152 | tf_op jit(solution)/shard_map/ppermute | solution.py:115
  25.7 8.2 %collective-permute-start.11 = (f32[1,512]{1,0:T(1,128)S(1)}, f32[1,512]{1,0:T(1,128)S(1)}, u32[]{:S(2)}, u32[]{:S(2)}) collective-permute-start(f32[1,512]{1,0:T(1,128)S(1)} %bitcast.30), channel_id=1, source_target_pairs={{0,1},{1,0},{2,3},{3,2},{4,5},{5,4},{6,7},{7,6},{8,9},{9,8},{10,11... | collective-permute-start | bytes 6152 | tf_op jit(solution)/shard_map/ppermute | solution.py:115
  33.9 102.4 %copy-start.25 = (f32[1,512]{1,0:T(1,128)}, f32[1,512]{1,0:T(1,128)S(1)}, u32[]{:S(2)}) copy-start(f32[1,512]{1,0:T(1,128)S(1)} %collective-permute-done.10.refs_13_) | copy-start | bytes 6148
  33.9 1.2 collective-permute-start.12
  33.9 102.3 %copy-start.26 = (f32[1,512]{1,0:T(1,128)}, f32[1,512]{1,0:T(1,128)S(1)}, u32[]{:S(2)}) copy-start(f32[1,512]{1,0:T(1,128)S(1)} %collective-permute-done.11.refs_14_) | copy-start | bytes 6148
  33.9 4.6 %collective-permute-start.2 = (bf16[768,256]{1,0:T(8,128)(2,1)}, bf16[768,256]{1,0:T(8,128)(2,1)S(1)}, u32[]{:S(2)}, u32[]{:S(2)}) collective-permute-start(bf16[768,256]{1,0:T(8,128)(2,1)} %attend.1.refs_0_), channel_id=1, source_target_pairs={{0,1},{1,0},{2,3},{3,2},{4,5},{5,4},{6,7},{7,6},{8,9},{9,8},{10,11... | collective-permute-start | bytes 1179656 | tf_op jit(solution)/shard_map/ppermute | solution.py:115
  35.1 101.2 %copy-start.27 = (f32[1,512]{1,0:T(1,128)}, f32[1,512]{1,0:T(1,128)S(1)}, u32[]{:S(2)}) copy-start(f32[1,512]{1,0:T(1,128)S(1)} %collective-permute-done.12.refs_15_) | copy-start | bytes 6148
  35.1 27.6 %collective-permute-start.13 = (bf16[768,256]{1,0:T(8,128)(2,1)}, bf16[768,256]{1,0:T(8,128)(2,1)S(1)}, u32[]{:S(2)}, u32[]{:S(2)}) collective-permute-start(bf16[768,256]{1,0:T(8,128)(2,1)} %attend.1.refs_0_), channel_id=1, source_target_pairs={{0,8},{8,0},{1,9},{9,1},{2,10},{10,2},{3,11},{11,3},{4,12},{12,4},... | collective-permute-start | bytes 1179656 | tf_op jit(solution)/shard_map/ppermute | solution.py:115
  35.6 41.8 %collective-permute-start.22 = (bf16[256,1408]{1,0:T(8,128)(2,1)}, bf16[256,1408]{1,0:T(8,128)(2,1)S(1)}, u32[]{:S(2)}, u32[]{:S(2)}) collective-permute-start(bf16[256,1408]{1,0:T(8,128)(2,1)} %get-tuple-element.16), channel_id=1, source_target_pairs={{0,8},{8,0},{1,9},{9,1},{2,10},{10,2},{3,11},{11,3},{4,12},{12,4},... | collective-permute-start | bytes 2162696 | tf_op jit(solution)/shard_map/ppermute | solution.py:115
  37.1 40.3 %collective-permute-start.24 = (bf16[256,1408]{1,0:T(8,128)(2,1)S(1)}, bf16[256,1408]{1,0:T(8,128)(2,1)S(1)}, u32[]{:S(2)}, u32[]{:S(2)}) collective-permute-start(bf16[256,1408]{1,0:T(8,128)(2,1)S(1)} %copy-done.3), channel_id=1, source_target_pairs={{0,16},{16,0},{1,17},{17,1},{2,18},{18,2},{3,19},{19,3},{4,20},{20... | collective-permute-start | bytes 2162696 | tf_op jit(solution)/shard_map/ppermute | solution.py:115
  38.6 38.9 %collective-permute-start.7 = (bf16[768,512]{1,0:T(8,128)(2,1)}, bf16[768,512]{1,0:T(8,128)(2,1)}, u32[]{:S(2)}, u32[]{:S(2)}) collective-permute-start(bf16[768,512]{1,0:T(8,128)(2,1)} %refs_8_.1), channel_id=1, source_target_pairs={{0,2},{2,0},{1,3},{3,1},{4,6},{6,4},{5,7},{7,5},{8,10},{10,8},{9,1... | collective-permute-start | bytes 2359304 | tf_op jit(solution)/shard_map/ppermute | solution.py:115
  62.7 70.9 %copy-start.18 = (bf16[768,256]{1,0:T(8,128)(2,1)}, bf16[768,256]{1,0:T(8,128)(2,1)S(1)}, u32[]{:S(2)}) copy-start(bf16[768,256]{1,0:T(8,128)(2,1)S(1)} %collective-permute-done.13.refs_0_) | copy-start | bytes 1179652
  62.7 15.2 %collective-permute-start.8 = (bf16[768,512]{1,0:T(8,128)(2,1)}, bf16[768,512]{1,0:T(8,128)(2,1)S(1)}, u32[]{:S(2)}, u32[]{:S(2)}) collective-permute-start(bf16[768,512]{1,0:T(8,128)(2,1)} %refs_8_.1), channel_id=1, source_target_pairs={{0,1},{1,0},{2,3},{3,2},{4,5},{5,4},{6,7},{7,6},{8,9},{9,8},{10,11... | collective-permute-start | bytes 2359304 | tf_op jit(solution)/shard_map/ppermute | solution.py:115
  62.8 83.4 %copy-start.5 = (bf16[256,1408]{1,0:T(8,128)(2,1)}, bf16[256,1408]{1,0:T(8,128)(2,1)S(1)}, u32[]{:S(2)}) copy-start(bf16[256,1408]{1,0:T(8,128)(2,1)S(1)} %collective-permute-done.21.refs_1_) | copy-start | bytes 2162692
  62.8 35.8 %collective-permute-start.4 = (bf16[256,2048]{1,0:T(8,128)(2,1)}, bf16[256,2048]{1,0:T(8,128)(2,1)}, u32[]{:S(2)}, u32[]{:S(2)}) collective-permute-start(bf16[256,2048]{1,0:T(8,128)(2,1)} %refs_4_.3), channel_id=1, source_target_pairs={{0,2},{2,0},{1,3},{3,1},{4,6},{6,4},{5,7},{7,5},{8,10},{10,8},{9,1... | collective-permute-start | bytes 3145736 | tf_op jit(solution)/shard_map/ppermute | solution.py:115
  77.4 19.2 %collective-permute-start.17 = (bf16[768,512]{1,0:T(8,128)(2,1)}, bf16[768,512]{1,0:T(8,128)(2,1)}, u32[]{:S(2)}, u32[]{:S(2)}) collective-permute-start(bf16[768,512]{1,0:T(8,128)(2,1)} %refs_8_.1), channel_id=1, source_target_pairs={{0,8},{8,0},{1,9},{9,1},{2,10},{10,2},{3,11},{11,3},{4,12},{12,4},... | collective-permute-start | bytes 2359304 | tf_op jit(solution)/shard_map/ppermute | solution.py:115
  77.4 22.7 %collective-permute-start.5 = (bf16[256,2048]{1,0:T(8,128)(2,1)}, bf16[256,2048]{1,0:T(8,128)(2,1)S(1)}, u32[]{:S(2)}, u32[]{:S(2)}) collective-permute-start(bf16[256,2048]{1,0:T(8,128)(2,1)} %refs_4_.3), channel_id=1, source_target_pairs={{0,1},{1,0},{2,3},{3,2},{4,5},{5,4},{6,7},{7,6},{8,9},{9,8},{10,11... | collective-permute-start | bytes 3145736 | tf_op jit(solution)/shard_map/ppermute | solution.py:115
  77.5 19.1 %collective-permute-start.3 = (bf16[768,256]{1,0:T(8,128)(2,1)S(1)}, bf16[768,256]{1,0:T(8,128)(2,1)S(1)}, u32[]{:S(2)}, u32[]{:S(2)}) collective-permute-start(bf16[768,256]{1,0:T(8,128)(2,1)S(1)} %collective-permute-done.1.refs_1_), channel_id=1, source_target_pairs={{0,1},{1,0},{2,3},{3,2},{4,5},{5,4},{6,7},{7,6},{8,9},{9,8},{10,11... | collective-permute-start | bytes 1179656 | tf_op jit(solution)/shard_map/ppermute | solution.py:115
  78.0 19.1 %collective-permute-start.14 = (bf16[768,256]{1,0:T(8,128)(2,1)S(1)}, bf16[768,256]{1,0:T(8,128)(2,1)}, u32[]{:S(2)}, u32[]{:S(2)}) collective-permute-start(bf16[768,256]{1,0:T(8,128)(2,1)S(1)} %collective-permute-done.13.refs_0_), channel_id=1, source_target_pairs={{0,2},{2,0},{1,3},{3,1},{4,6},{6,4},{5,7},{7,5},{8,10},{10,8},{9,1... | collective-permute-start | bytes 1179656 | tf_op jit(solution)/shard_map/ppermute | solution.py:115
  96.6 2.2 collective-permute-start.15
  96.6 38.4 %collective-permute-start.9 = (bf16[768,512]{1,0:T(8,128)(2,1)}, bf16[768,512]{1,0:T(8,128)(2,1)}, u32[]{:S(2)}, u32[]{:S(2)}) collective-permute-start(bf16[768,512]{1,0:T(8,128)(2,1)} %collective-permute-done.7.refs_9_), channel_id=1, source_target_pairs={{0,1},{1,0},{2,3},{3,2},{4,5},{5,4},{6,7},{7,6},{8,9},{9,8},{10,11... | collective-permute-start | bytes 2359304 | tf_op jit(solution)/shard_map/ppermute | solution.py:115
  97.1 37.9 %collective-permute-start.18 = (bf16[768,512]{1,0:T(8,128)(2,1)}, bf16[768,512]{1,0:T(8,128)(2,1)}, u32[]{:S(2)}, u32[]{:S(2)}) collective-permute-start(bf16[768,512]{1,0:T(8,128)(2,1)} %collective-permute-done.17.refs_8_), channel_id=1, source_target_pairs={{0,2},{2,0},{1,3},{3,1},{4,6},{6,4},{5,7},{7,5},{8,10},{10,8},{9,1... | collective-permute-start | bytes 2359304 | tf_op jit(solution)/shard_map/ppermute | solution.py:115
  98.6 37.6 %collective-permute-start.6 = (bf16[256,2048]{1,0:T(8,128)(2,1)}, bf16[256,2048]{1,0:T(8,128)(2,1)}, u32[]{:S(2)}, u32[]{:S(2)}) collective-permute-start(bf16[256,2048]{1,0:T(8,128)(2,1)} %collective-permute-done.4.refs_5_), channel_id=1, source_target_pairs={{0,1},{1,0},{2,3},{3,2},{4,5},{5,4},{6,7},{7,6},{8,9},{9,8},{10,11... | collective-permute-start | bytes 3145736 | tf_op jit(solution)/shard_map/ppermute | solution.py:115
  98.8 27.2 %collective-permute-start.26 = (bf16[128,1408]{1,0:T(8,128)(2,1)S(1)}, bf16[128,1408]{1,0:T(8,128)(2,1)}, u32[]{:S(2)}, u32[]{:S(2)}) collective-permute-start(bf16[128,1408]{1,0:T(8,128)(2,1)S(1)} %get-tuple-element.24), channel_id=1, source_target_pairs={{0,16},{16,0},{1,17},{17,1},{2,18},{18,2},{3,19},{19,3},{4,20},{20... | collective-permute-start | bytes 1081352 | tf_op jit(solution)/shard_map/ppermute | solution.py:115
  100.1 33.5 %collective-permute-start.27 = (bf16[128,1408]{1,0:T(8,128)(2,1)S(1)}, bf16[128,1408]{1,0:T(8,128)(2,1)}, u32[]{:S(2)}, u32[]{:S(2)}) collective-permute-start(bf16[128,1408]{1,0:T(8,128)(2,1)S(1)} %get-tuple-element.23), channel_id=1, source_target_pairs={{0,16},{16,0},{1,17},{17,1},{2,18},{18,2},{3,19},{19,3},{4,20},{20... | collective-permute-start | bytes 1081352 | tf_op jit(solution)/shard_map/ppermute | solution.py:115
  126.0 20.2 %collective-permute-start.23 = (bf16[256,1408]{1,0:T(8,128)(2,1)S(1)}, bf16[256,1408]{1,0:T(8,128)(2,1)S(1)}, u32[]{:S(2)}, u32[]{:S(2)}) collective-permute-start(bf16[256,1408]{1,0:T(8,128)(2,1)S(1)} %collective-permute-done.22.refs_2_), channel_id=1, source_target_pairs={{0,4},{4,0},{1,5},{5,1},{2,6},{6,2},{3,7},{7,3},{8,12},{12,8},{9,1... | collective-permute-start | bytes 2162696 | tf_op jit(solution)/shard_map/ppermute | solution.py:115
  133.7 26.9 %collective-permute-start.25 = (bf16[256,1408]{1,0:T(8,128)(2,1)S(1)}, bf16[256,1408]{1,0:T(8,128)(2,1)}, u32[]{:S(2)}, u32[]{:S(2)}) collective-permute-start(bf16[256,1408]{1,0:T(8,128)(2,1)S(1)} %collective-permute-done.24.refs_4_), channel_id=1, source_target_pairs={{0,4},{4,0},{1,5},{5,1},{2,6},{6,2},{3,7},{7,3},{8,12},{12,8},{9,1... | collective-permute-start | bytes 2162696 | tf_op jit(solution)/shard_map/ppermute | solution.py:115
  134.9 35.4 %collective-permute-start.19 = (bf16[768,512]{1,0:T(8,128)(2,1)}, bf16[768,512]{1,0:T(8,128)(2,1)}, u32[]{:S(2)}, u32[]{:S(2)}) collective-permute-start(bf16[768,512]{1,0:T(8,128)(2,1)} %collective-permute-done.17.refs_8_), channel_id=1, source_target_pairs={{0,1},{1,0},{2,3},{3,2},{4,5},{5,4},{6,7},{7,6},{8,9},{9,8},{10,11... | collective-permute-start | bytes 2359304 | tf_op jit(solution)/shard_map/ppermute | solution.py:115
  135.0 38.3 %collective-permute-start.20 = (bf16[768,512]{1,0:T(8,128)(2,1)}, bf16[768,512]{1,0:T(8,128)(2,1)}, u32[]{:S(2)}, u32[]{:S(2)}) collective-permute-start(bf16[768,512]{1,0:T(8,128)(2,1)} %collective-permute-done.18.refs_9_), channel_id=1, source_target_pairs={{0,1},{1,0},{2,3},{3,2},{4,5},{5,4},{6,7},{7,6},{8,9},{9,8},{10,11... | collective-permute-start | bytes 2359304 | tf_op jit(solution)/shard_map/ppermute | solution.py:115
  136.2 34.1 %collective-permute-start.16 = (bf16[768,256]{1,0:T(8,128)(2,1)}, bf16[768,256]{1,0:T(8,128)(2,1)}, u32[]{:S(2)}, u32[]{:S(2)}) collective-permute-start(bf16[768,256]{1,0:T(8,128)(2,1)} %collective-permute-done.14.refs_1_), channel_id=1, source_target_pairs={{0,1},{1,0},{2,3},{3,2},{4,5},{5,4},{6,7},{7,6},{8,9},{9,8},{10,11... | collective-permute-start | bytes 1179656 | tf_op jit(solution)/shard_map/ppermute | solution.py:115
  146.2 36.9 %collective-permute-start.28 = (bf16[128,1408]{1,0:T(8,128)(2,1)}, bf16[128,1408]{1,0:T(8,128)(2,1)}, u32[]{:S(2)}, u32[]{:S(2)}) collective-permute-start(bf16[128,1408]{1,0:T(8,128)(2,1)} %collective-permute-done.26.refs_6_), channel_id=1, source_target_pairs={{0,4},{4,0},{1,5},{5,1},{2,6},{6,2},{3,7},{7,3},{8,12},{12,8},{9,1... | collective-permute-start | bytes 1081352 | tf_op jit(solution)/shard_map/ppermute | solution.py:115
  160.5 22.6 %collective-permute-start.29 = (bf16[128,1408]{1,0:T(8,128)(2,1)}, bf16[128,1408]{1,0:T(8,128)(2,1)}, u32[]{:S(2)}, u32[]{:S(2)}) collective-permute-start(bf16[128,1408]{1,0:T(8,128)(2,1)} %collective-permute-done.27.refs_7_), channel_id=1, source_target_pairs={{0,4},{4,0},{1,5},{5,1},{2,6},{6,2},{3,7},{7,3},{8,12},{12,8},{9,1... | collective-permute-start | bytes 1081352 | tf_op jit(solution)/shard_map/ppermute | solution.py:115
  170.3 29.3 %collective-permute-start.31 = (bf16[704,256]{1,0:T(8,128)(2,1)S(1)}, bf16[704,256]{1,0:T(8,128)(2,1)S(1)}, u32[]{:S(2)}, u32[]{:S(2)}) collective-permute-start(bf16[704,256]{1,0:T(8,128)(2,1)S(1)} %copy-done), channel_id=1, source_target_pairs={{0,16},{16,0},{1,17},{17,1},{2,18},{18,2},{3,19},{19,3},{4,20},{20... | collective-permute-start | bytes 1081352 | tf_op jit(solution)/shard_map/ppermute | solution.py:115
  170.4 32.1 %collective-permute-start.32 = (bf16[704,256]{1,0:T(8,128)(2,1)S(1)}, bf16[704,256]{1,0:T(8,128)(2,1)S(1)}, u32[]{:S(2)}, u32[]{:S(2)}) collective-permute-start(bf16[704,256]{1,0:T(8,128)(2,1)S(1)} %collective-permute-done.30.refs_1_), channel_id=1, source_target_pairs={{0,16},{16,0},{1,17},{17,1},{2,18},{18,2},{3,19},{19,3},{4,20},{20... | collective-permute-start | bytes 1081352 | tf_op jit(solution)/shard_map/ppermute | solution.py:115
  205.0 36.9 %collective-permute-start.33 = (bf16[1536,512]{1,0:T(8,128)(2,1)S(1)}, bf16[1536,512]{1,0:T(8,128)(2,1)S(1)}, u32[]{:S(2)}, u32[]{:S(2)}) collective-permute-start(bf16[1536,512]{1,0:T(8,128)(2,1)S(1)} %shard_map.123), channel_id=1, source_target_pairs={{0,1},{1,0},{2,3},{3,2},{4,5},{5,4},{6,7},{7,6},{8,9},{9,8},{10,11... | collective-permute-start | bytes 4718600 | tf_op jit(solution)/shard_map/ppermute | solution.py:115
  205.1 11.4 %collective-permute-start.36 = (bf16[704,256]{1,0:T(8,128)(2,1)S(1)}, bf16[704,256]{1,0:T(8,128)(2,1)S(1)}, u32[]{:S(2)}, u32[]{:S(2)}) collective-permute-start(bf16[704,256]{1,0:T(8,128)(2,1)S(1)} %copy-done), channel_id=1, source_target_pairs={{0,4},{4,0},{1,5},{5,1},{2,6},{6,2},{3,7},{7,3},{8,12},{12,8},{9,1... | collective-permute-start | bytes 1081352 | tf_op jit(solution)/shard_map/ppermute | solution.py:115
  206.7 17.5 %collective-permute-start.37 = (bf16[704,256]{1,0:T(8,128)(2,1)S(1)}, bf16[704,256]{1,0:T(8,128)(2,1)S(1)}, u32[]{:S(2)}, u32[]{:S(2)}) collective-permute-start(bf16[704,256]{1,0:T(8,128)(2,1)S(1)} %collective-permute-done.30.refs_1_), channel_id=1, source_target_pairs={{0,4},{4,0},{1,5},{5,1},{2,6},{6,2},{3,7},{7,3},{8,12},{12,8},{9,1... | collective-permute-start | bytes 1081352 | tf_op jit(solution)/shard_map/ppermute | solution.py:115
  207.2 24.7 %collective-permute-start.38 = (bf16[704,256]{1,0:T(8,128)(2,1)S(1)}, bf16[704,256]{1,0:T(8,128)(2,1)S(1)}, u32[]{:S(2)}, u32[]{:S(2)}) collective-permute-start(bf16[704,256]{1,0:T(8,128)(2,1)S(1)} %collective-permute-done.31.refs_2_), channel_id=1, source_target_pairs={{0,4},{4,0},{1,5},{5,1},{2,6},{6,2},{3,7},{7,3},{8,12},{12,8},{9,1... | collective-permute-start | bytes 1081352 | tf_op jit(solution)/shard_map/ppermute | solution.py:115
  208.7 30.4 %collective-permute-start.39 = (bf16[704,256]{1,0:T(8,128)(2,1)S(1)}, bf16[704,256]{1,0:T(8,128)(2,1)S(1)}, u32[]{:S(2)}, u32[]{:S(2)}) collective-permute-start(bf16[704,256]{1,0:T(8,128)(2,1)S(1)} %collective-permute-done.32.refs_3_), channel_id=1, source_target_pairs={{0,4},{4,0},{1,5},{5,1},{2,6},{6,2},{3,7},{7,3},{8,12},{12,8},{9,1... | collective-permute-start | bytes 1081352 | tf_op jit(solution)/shard_map/ppermute | solution.py:115
  241.8 3.5 %collective-permute-start.40 = (bf16[1536,512]{1,0:T(8,128)(2,1)S(1)}, bf16[1536,512]{1,0:T(8,128)(2,1)S(1)}, u32[]{:S(2)}, u32[]{:S(2)}) collective-permute-start(bf16[1536,512]{1,0:T(8,128)(2,1)S(1)} %shard_map.125), channel_id=1, source_target_pairs={{0,1},{1,0},{2,3},{3,2},{4,5},{5,4},{6,7},{7,6},{8,9},{9,8},{10,11... | collective-permute-start | bytes 4718600 | tf_op jit(solution)/shard_map/ppermute | solution.py:115
  244.5 20.0 %collective-permute-start.34 = (bf16[768,512]{1,0:T(8,128)(2,1)S(1)}, bf16[768,512]{1,0:T(8,128)(2,1)S(1)}, u32[]{:S(2)}, u32[]{:S(2)}) collective-permute-start(bf16[768,512]{1,0:T(8,128)(2,1)S(1)} %slice.55), channel_id=1, source_target_pairs={{0,8},{8,0},{1,9},{9,1},{2,10},{10,2},{3,11},{11,3},{4,12},{12,4},... | collective-permute-start | bytes 2359304 | tf_op jit(solution)/shard_map/ppermute | solution.py:115
  247.9 19.6 %collective-permute-start.41 = (bf16[1536,256]{1,0:T(8,128)(2,1)S(1)}, bf16[1536,256]{1,0:T(8,128)(2,1)S(1)}, u32[]{:S(2)}, u32[]{:S(2)}) collective-permute-start(bf16[1536,256]{1,0:T(8,128)(2,1)S(1)} %slice.59), channel_id=1, source_target_pairs={{0,2},{2,0},{1,3},{3,1},{4,6},{6,4},{5,7},{7,5},{8,10},{10,8},{9,1... | collective-permute-start | bytes 2359304 | tf_op jit(solution)/shard_map/ppermute | solution.py:115
  265.6 10.6 %collective-permute-start.35 = (bf16[768,256]{1,0:T(8,128)(2,1)S(1)}, bf16[768,256]{1,0:T(8,128)(2,1)S(1)}, u32[]{:S(2)}, u32[]{:S(2)}) collective-permute-start(bf16[768,256]{1,0:T(8,128)(2,1)S(1)} %get-tuple-element.21), channel_id=1, source_target_pairs={{0,2},{2,0},{1,3},{3,1},{4,6},{6,4},{5,7},{7,5},{8,10},{10,8},{9,1... | collective-permute-start | bytes 1179656 | tf_op jit(solution)/shard_map/ppermute | solution.py:115
  268.6 10.3 %collective-permute-start.42 = (bf16[768,256]{1,0:T(8,128)(2,1)S(1)}, bf16[768,256]{1,0:T(8,128)(2,1)S(1)}, u32[]{:S(2)}, u32[]{:S(2)}) collective-permute-start(bf16[768,256]{1,0:T(8,128)(2,1)S(1)} %get-tuple-element.19), channel_id=1, source_target_pairs={{0,8},{8,0},{1,9},{9,1},{2,10},{10,2},{3,11},{11,3},{4,12},{12,4},... | collective-permute-start | bytes 1179656 | tf_op jit(solution)/shard_map/ppermute | solution.py:115
  (23 other events, 400.9 us)
where the time goes:
time: 283 us; the launch traced here: 282 us
  waiting for transfers between devices  165 us (58%)
  Pallas kernels  65.2 us (23%)
  starting transfers between devices  38.3 us (14%)
  local copies, waits for them, and re-layouts  12.1 us (4%)
    ppermute x42, waiting for transfers between devices, swap(): return lax.ppermute(block, axis, [(0, 1), (1, 0)])  165 us
    ppermute x42, starting transfers between devices, swap(): return lax.ppermute(block, axis, [(0, 1), (1, 0)])  33.4 us
    pallas_call x2, Pallas kernels, project(): pl.pallas_call(project_kernel, grid_spec=pltpu.PrefetchScalarGridSpec(num...  19.7 us
    pallas_call x1, Pallas kernels, hidden_units(): pl.pallas_call(functools.partial(hidden_kernel, main, tail, early, len(pi...  10.4 us
    pallas_call x4, Pallas kernels, down(): pl.pallas_call(functools.partial(down_kernel, bool(got)), grid_spec=pltpu...  10.4 us
    pallas_call x1, Pallas kernels, partial_acts(): pl.pallas_call(functools.partial(partial_kernel, count), grid_spec=pltpu....  9.21 us
    pallas_call x1, Pallas kernels, attend(): pl.pallas_call(attend_kernel, grid_spec=pltpu.PrefetchScalarGridSpec(num_...  8.3 us
    unnamed x56, local copies, waits for them, and re-layouts  7.42 us
  transfers between devices with their start and end apart: 43, of which 18 were waited for; matrix products, arithmetic and copies ran while one was open for 2% of the time, Pallas kernels for 21%

commit v1 on v0

--- a/solution.py
+++ b/solution.py
@@ -13,6 +13,7 @@
 EPS = 1e-06
 LANES = 128
 MIB = 2**20
+PROJECT_MIB, PARTIAL_MIB, HIDDEN_MIB, NEAR_MIB, DOWN_MIB = 60, 60, 56, 56, 24
 
 
 def from_behind(block, axes, count):
@@ -192,20 +193,24 @@
     )(place, sinks, queries, keys, values, halo, *gains)
 
 
-def halves_kernel(main, tail, place_ref, gate_ref, up_ref, own_ref, far_ref):
-    def put(ref, h):
-        ref[:, :main] = gate_ref[:, h * main : (h + 1) * main]
-        ref[:, main : 2 * main] = up_ref[:, h * main : (h + 1) * main]
-        if tail:
-            rest = [r[:, 2 * main :][:, h * tail : (h + 1) * tail] for r in (gate_ref, up_ref)]
-            ref[:, 2 * main :] = jnp.concatenate(rest, axis=1)
+def halves_kernel(main, tail, place_ref, gate_ref, up_ref, *outs):
+    def put(refs, h):
+        start = 0
+        for ref in refs:
+            rows = slice(start, start + ref.shape[0])
+            start += ref.shape[0]
+            ref[:, :main] = gate_ref[rows, h * main : (h + 1) * main]
+            ref[:, main : 2 * main] = up_ref[rows, h * main : (h + 1) * main]
+            if tail:
+                rest = [r[rows, 2 * main :][:, h * tail :][:, :tail] for r in (gate_ref, up_ref)]
+                ref[:, 2 * main :] = jnp.concatenate(rest, axis=1)
 
     for low in (0, 1):
 
         @pl.when(place_ref[0] == low)
         def _():
-            put(own_ref, low)
-            put(far_ref, 1 - low)
+            put(outs[:1], low)
+            put(outs[1:], 1 - low)
 
 
 def down_halves_kernel(main, tail, place_ref, down_ref, own_ref, far_ref):
@@ -222,7 +227,7 @@
             put(far_ref, 1 - low)
 
 
-def split(kernel, place, shape, *weights):
+def split(kernel, place, shapes, *weights):
     spec = lambda s: pl.BlockSpec(s, lambda i, p: (0, 0))
     return pl.pallas_call(
         kernel,
@@ -230,18 +235,15 @@
             num_scalar_prefetch=1,
             grid=(1,),
             in_specs=[spec(w.shape) for w in weights],
-            out_specs=[spec(shape)] * 2,
-        ),
-        out_shape=[jax.ShapeDtypeStruct(shape, jnp.bfloat16)] * 2,
+            out_specs=[spec(s) for s in shapes],
+        ),
+        out_shape=[jax.ShapeDtypeStruct(s, jnp.bfloat16) for s in shapes],
         cost_estimate=pl.CostEstimate(flops=10**9, bytes_accessed=10**6, transcendentals=0),
     )(place, *weights)
 
 
-def project_kernel(place_ref, *refs):
-    atts, outs, ress, gains = (refs[4 * n : 4 * n + 4] for n in range(4))
-    normed_ref, middle_ref, held = refs[16:]
+def normed_rows(columns, atts, outs, ress, gains, held, normed_ref):
     width = ress[0].shape[1]
-    columns = [pl.ds(pl.multiple_of(place_ref[n] * width, width), width) for n in range(4)]
     squares = 0.0
     for n in range(4):
         total = sum(
@@ -256,6 +258,19 @@
     for n in range(4):
         wide = held[n].astype(jnp.float32)
         normed_ref[:, columns[n]] = (wide * scale * gains[n][...]).astype(jnp.bfloat16)
+
+
+def spans(place_ref, first, count, width):
+    return [
+        pl.ds(pl.multiple_of(place_ref[first + n] * width, width), width) for n in range(count)
+    ]
+
+
+def project_kernel(place_ref, *refs):
+    atts, outs, ress, gains = (refs[4 * n : 4 * n + 4] for n in range(4))
+    normed_ref, middle_ref, held = refs[16:]
+    columns = spans(place_ref, 0, 4, ress[0].shape[1])
+    normed_rows(columns, atts, outs, ress, gains, held, normed_ref)
     middle_ref[...] = held[0]
 
 
@@ -281,112 +296,116 @@
             jax.ShapeDtypeStruct((rows, width), jnp.bfloat16),
             jax.ShapeDtypeStruct((rows, part), jnp.bfloat16),
         ],
-        compiler_params=pltpu.CompilerParams(vmem_limit_bytes=60 * MIB),
+        compiler_params=pltpu.CompilerParams(vmem_limit_bytes=PROJECT_MIB * MIB),
         cost_estimate=pl.CostEstimate(
             flops=8 * rows * depth * width, bytes_accessed=4 * rows * width, transcendentals=0
         ),
     )(place, *atts, *outs, *ress, *gains)
 
 
+def stack_pieces(pieces, whole):
+    start = 0
+    for piece in pieces:
+        whole[start : start + piece.shape[0], :] = piece[...]
+        start += piece.shape[0]
+
+
+def put_hidden(main, tail, acts, out_ref):
+    def gated(gate, up):
+        return (gate / (1.0 + jnp.exp(-gate)) * up).astype(jnp.bfloat16)
+
+    out_ref[:, :main] = gated(acts[:, :main], acts[:, main : 2 * main])
+    if tail:
+        rest = acts[:, 2 * main :]
+        out_ref[:, main:] = gated(rest[:, :tail], rest[:, tail:])
+
+
+def product(columns, x_ref, whole):
+    x = jnp.concatenate([x_ref[:, c] for c in columns], axis=1)
+    return jnp.dot(x, whole[...], preferred_element_type=jnp.float32)
+
+
+def far_kernel(main, tail, count, place_ref, *refs):
+    atts, outs, ress, gains = (refs[4 * n : 4 * n + 4] for n in range(4))
+    pieces, (out_ref, whole, held, x_ref) = refs[16 : 16 + count], refs[16 + count :]
+    pl.when(pl.program_id(0) == 0)(lambda: stack_pieces(pieces, whole))
+    columns = spans(place_ref, 0, 4, ress[0].shape[1])
+    normed_rows(columns, atts, outs, ress, gains, held, x_ref)
+    acts = product(spans(place_ref, 4, 8, x_ref.shape[1] // 8), x_ref, whole)
+    put_hidden(main, tail, acts, out_ref)
+
+
+def far_hidden(place, atts, outs, ress, gains, pieces, main, tail, tile):
+    rows, part = ress[0].shape
+    depth = sum(p.shape[0] for p in pieces)
+    width = pieces[0].shape[1]
+    tiles = rows // tile
+    row_spec = lambda a: pl.BlockSpec((tile, a.shape[1]), lambda i, p: (i, 0))
+    full = lambda a: pl.BlockSpec(a.shape, lambda i, p: (0, 0), pipeline_mode=pl.Buffered(1))
+    operands = [*atts, *outs, *ress, *gains, *pieces]
+    specs = [*map(row_spec, atts), *map(full, outs), *map(row_spec, ress)]
+    return pl.pallas_call(
+        functools.partial(far_kernel, main, tail, len(pieces)),
+        grid_spec=pltpu.PrefetchScalarGridSpec(
+            num_scalar_prefetch=1,
+            grid=(tiles,),
+            in_specs=[*specs, *map(full, [*gains, *pieces])],
+            out_specs=pl.BlockSpec((tile, main + tail), lambda i, p: (i, 0)),
+            scratch_shapes=[
+                pltpu.VMEM((depth, width), jnp.bfloat16),
+                pltpu.VMEM((4, tile, part), jnp.bfloat16),
+                pltpu.VMEM((tile, depth), jnp.bfloat16),
+            ],
+        ),
+        out_shape=jax.ShapeDtypeStruct((rows, main + tail), jnp.bfloat16),
+        compiler_params=pltpu.CompilerParams(vmem_limit_bytes=HIDDEN_MIB * MIB),
+        cost_estimate=pl.CostEstimate(
+            flops=4 * rows * depth * width, bytes_accessed=8 * rows * width, transcendentals=0
+        ),
+        name="far_hidden",
+    )(place, *operands)
+
+
 def partial_kernel(count, place_ref, x_ref, *refs):
     pieces, out_ref, whole = refs[:count], refs[count], refs[count + 1]
-    depth = pieces[0].shape[0]
-
-    @pl.when(pl.program_id(0) == 0)
-    def _():
-        for n, piece in enumerate(pieces):
-            whole[n * depth : (n + 1) * depth, :] = piece[...]
-
-    columns = [pl.ds(pl.multiple_of(place_ref[n] * depth, depth), depth) for n in range(count)]
-    x = jnp.concatenate([x_ref[:, c] for c in columns], axis=1)
-    out_ref[...] = jnp.dot(x, whole[...], preferred_element_type=jnp.float32)
-
-
-def partial_acts(place, x, pieces, tile):
-    rows, depth = x.shape
-    count, (piece, width) = len(pieces), pieces[0].shape
+    pl.when(pl.program_id(0) == 0)(lambda: stack_pieces(pieces, whole))
+    depth = x_ref.shape[1] // 8
+    columns = spans(place_ref, 4, whole.shape[0] // depth, depth)
+    out_ref[...] = product(columns, x_ref, whole)
+
+
+def near_kernel(main, tail, count, place_ref, x_ref, acts_ref, *refs):
+    pieces, (out_ref, whole) = refs[:count], refs[count:]
+    pl.when(pl.program_id(0) == 0)(lambda: stack_pieces(pieces, whole))
+    depth = x_ref.shape[1] // 8
+    blocks = whole.shape[0] // depth
+    columns = spans(place_ref, 12 - blocks, blocks, depth)
+    put_hidden(main, tail, acts_ref[...] + product(columns, x_ref, whole), out_ref)
+
+
+def near_step(kernel, place, x, more, pieces, out_shape, limit, tile):
+    rows, _ = x.shape
+    total = sum(p.shape[0] for p in pieces)
+    row_spec = lambda a: pl.BlockSpec((tile, a.shape[1]), lambda i, p: (i, 0))
+    full = lambda a: pl.BlockSpec(a.shape, lambda i, p: (0, 0), pipeline_mode=pl.Buffered(1))
     return pl.pallas_call(
-        functools.partial(partial_kernel, count),
+        kernel,
         grid_spec=pltpu.PrefetchScalarGridSpec(
             num_scalar_prefetch=1,
             grid=(rows // tile,),
-            in_specs=[pl.BlockSpec((tile, depth), lambda i, p: (i, 0))]
-            + [pl.BlockSpec(p.shape, lambda i, p: (0, 0)) for p in pieces],
-            out_specs=pl.BlockSpec((tile, width), lambda i, p: (i, 0)),
-            scratch_shapes=[pltpu.VMEM((count * piece, width), jnp.bfloat16)],
-        ),
-        out_shape=jax.ShapeDtypeStruct((rows, width), jnp.float32),
-        compiler_params=pltpu.CompilerParams(vmem_limit_bytes=60 * MIB),
+            in_specs=[row_spec(x), *map(row_spec, more), *map(full, pieces)],
+            out_specs=row_spec(out_shape),
+            scratch_shapes=[pltpu.VMEM((total, pieces[0].shape[1]), jnp.bfloat16)],
+        ),
+        out_shape=out_shape,
+        compiler_params=pltpu.CompilerParams(vmem_limit_bytes=limit * MIB),
         cost_estimate=pl.CostEstimate(
-            flops=2 * rows * count * piece * width, bytes_accessed=4 * rows * width,
-            transcendentals=0,
-        ),
-    )(place, x, *pieces)
-
-
-def hidden_kernel(main, tail, early, count, place_ref, near_ref, far_ref, acts_ref, *refs):
-    pieces, out_ref, whole = refs[:count], refs[count], refs[count + 1]
-    depth = near_ref.shape[1] // 8
-    step = pl.program_id(0)
-    middle = pl.num_programs(0) // 2
-
-    @pl.when(step == 0)
-    def _():
-        start = 0
-        for piece in pieces:
-            whole[start : start + piece.shape[0], :] = piece[...]
-            start += piece.shape[0]
-
-    def gated(gate, up):
-        return (gate / (1.0 + jnp.exp(-gate)) * up).astype(jnp.bfloat16)
-
-    def product(x_ref, first):
-        columns = [
-            pl.ds(pl.multiple_of(place_ref[n] * depth, depth), depth) for n in range(first, 8)
-        ]
-        x = jnp.concatenate([x_ref[:, c] for c in columns], axis=1)
-        return jnp.dot(x, whole[first * depth :, :], preferred_element_type=jnp.float32)
-
-    def finish(acts):
-        out_ref[:, :main] = gated(acts[:, :main], acts[:, main : 2 * main])
-        if tail:
-            rest = acts[:, 2 * main :]
-            out_ref[:, main:] = gated(rest[:, :tail], rest[:, tail:])
-
-    pl.when(step < middle)(lambda: finish(acts_ref[...] + product(near_ref, early)))
-    pl.when(step >= middle)(lambda: finish(product(far_ref, 0)))
-
-
-def hidden_units(place, near, far, acts, pieces, early, main, tail, tile):
-    rows, depth = near.shape
-    width = pieces[0].shape[1]
-    tiles = rows // tile
-    first = lambda i, p: (jnp.minimum(i, tiles - 1), 0)
-    second = lambda i, p: (jnp.maximum(i - tiles, 0), 0)
-    return pl.pallas_call(
-        functools.partial(hidden_kernel, main, tail, early, len(pieces)),
-        grid_spec=pltpu.PrefetchScalarGridSpec(
-            num_scalar_prefetch=1,
-            grid=(2 * tiles,),
-            in_specs=[
-                pl.BlockSpec((tile, depth), first),
-                pl.BlockSpec((tile, depth), second),
-                pl.BlockSpec((tile, width), first),
-            ]
-            + [pl.BlockSpec(p.shape, lambda i, p: (0, 0)) for p in pieces],
-            out_specs=pl.BlockSpec((tile, main + tail), lambda i, p: (i, 0)),
-            scratch_shapes=[pltpu.VMEM((depth, width), jnp.bfloat16)],
-        ),
-        out_shape=jax.ShapeDtypeStruct((2 * rows, main + tail), jnp.bfloat16),
-        compiler_params=pltpu.CompilerParams(vmem_limit_bytes=40 * MIB),
-        cost_estimate=pl.CostEstimate(
-            flops=3 * rows * depth * width, bytes_accessed=8 * rows * width, transcendentals=0
-        ),
-        name="hidden_units",
-    )(place, near, far, acts, *pieces)
-
-
-def down_kernel(kept, flag_ref, hidden_ref, *refs):
+            flops=3000 * rows * total, bytes_accessed=4000 * rows, transcendentals=0
+        ),
+    )(place, x, *more, *pieces)
+
+
+def down_kernel(kept, flag_ref, near_ref, far_ref, *refs):
     pieces, (*got_ref, out_ref, whole) = refs[:4], refs[4:]
     block = pieces[0].shape[1]
 
@@ -402,33 +421,36 @@
                             at = block if (n // 2) == near else 0
                             whole[:, at : at + block] = piece[...]
 
-    acts = jnp.dot(hidden_ref[...], whole[...], preferred_element_type=jnp.float32)
-    if kept:
-        acts += got_ref[0][...].astype(jnp.float32)
-    out_ref[...] = acts.astype(jnp.bfloat16)
-
-
-def down(flags, hidden, pieces, tile, got=()):
-    rows, depth = hidden.shape
+    def put(hidden_ref):
+        acts = jnp.dot(hidden_ref[...], whole[...], preferred_element_type=jnp.float32)
+        if kept:
+            acts += got_ref[0][...].astype(jnp.float32)
+        out_ref[...] = acts.astype(jnp.bfloat16)
+
+    pl.when(pl.program_id(0) == 0)(lambda: put(near_ref))
+    pl.when(pl.program_id(0) == 1)(lambda: put(far_ref))
+
+
+def down(flags, near, far, pieces, got=()):
+    rows, depth = near.shape
     block = pieces[0].shape[1]
-    row_spec = lambda n: pl.BlockSpec((tile, n), lambda i, p: (i, 0))
+    row_spec = pl.BlockSpec((rows, 2 * block), lambda i, p: (i, 0))
+    full = lambda a: pl.BlockSpec(a.shape, lambda i, p: (0, 0))
     return pl.pallas_call(
         functools.partial(down_kernel, bool(got)),
         grid_spec=pltpu.PrefetchScalarGridSpec(
             num_scalar_prefetch=1,
-            grid=(rows // tile,),
-            in_specs=[row_spec(depth)]
-            + [pl.BlockSpec(p.shape, lambda i, p: (0, 0)) for p in pieces]
-            + [row_spec(2 * block)] * len(got),
-            out_specs=row_spec(2 * block),
+            grid=(2,),
+            in_specs=[full(near), full(far), *map(full, pieces)] + [row_spec] * len(got),
+            out_specs=row_spec,
             scratch_shapes=[pltpu.VMEM((depth, 2 * block), jnp.bfloat16)],
         ),
-        out_shape=jax.ShapeDtypeStruct((rows, 2 * block), jnp.bfloat16),
-        compiler_params=pltpu.CompilerParams(vmem_limit_bytes=20 * MIB),
+        out_shape=jax.ShapeDtypeStruct((2 * rows, 2 * block), jnp.bfloat16),
+        compiler_params=pltpu.CompilerParams(vmem_limit_bytes=DOWN_MIB * MIB),
         cost_estimate=pl.CostEstimate(
-            flops=4 * rows * depth * block, bytes_accessed=4 * rows * block, transcendentals=0
-        ),
-    )(flags, hidden, *pieces, *got)
+            flops=8 * rows * depth * block, bytes_accessed=8 * rows * block, transcendentals=0
+        ),
+    )(flags, near, far, *pieces, *got)
 
 
 def finish_kernel(flag_ref, middle_ref, ahead_ref, ahead_got, behind_ref, behind_got, out_ref):
@@ -484,26 +506,27 @@
     edge = jnp.concatenate([keys[:, rows - WINDOW :], values[:, rows - WINDOW :]], axis=0)
     halo = from_behind(edge, sp_axes, lax.axis_size(sp_axes))
 
-    gu_own, gu_far = split(
+    depth = gate_weight.shape[0]
+    gu_own, *gu_far = split(
         functools.partial(halves_kernel, main, tail), one(zl),
-        gate_weight.shape, gate_weight, up_weight,
-    )
-    gu_swp = swap(gu_far, "zl")
+        [(depth, units), (depth // 2, units), (depth // 2, units)], gate_weight, up_weight,
+    )
+    pair = lambda parts, axis: [swap(parts[n], axis) for n in (0, 1)]
+    gu_swp = pair(gu_far, "zl")
     gu_own_m = swap(gu_own, "zh")
     gu_own_y = swap(gu_own, "y")
     res2 = swap(residual, "zl")
     dn_own, dn_far = split(
         functools.partial(down_halves_kernel, main, tail), one(zl),
-        (main + tail, block), down_weight,
+        [(main + tail, block)] * 2, down_weight,
     )
     attended = attend(
         one(lax.axis_index(sp_axes)), sink_logits, queries, keys, values, halo, query_gain,
         key_gain,
     )
     att2 = swap(attended, "zl")
-    part = gu_swp.shape[0] // 2
-    gu_swp_m = [swap(gu_swp[n * part : (n + 1) * part], "zh") for n in (0, 1)]
-    gu_swp_y = swap(gu_swp, "y")
+    gu_swp_m = pair(gu_swp, "zh")
+    gu_swp_y = pair(gu_swp, "y")
     dn_swp = swap(dn_far, "zl")
     dn_own_m = swap(dn_own, "zh")
     dn_own_y = swap(dn_own, "y")
@@ -521,32 +544,41 @@
     outs = over_tp(out_weight)
     normed, middle = project(
         place, over_tp(attended), outs, over_tp(residual), gains,
-        256,
-    )
-    normed2, _ = project(place, over_tp(att2), outs, over_tp(res2), gains, 256)
-
-    gu_swp_my = [swap(gu_swp_m[n], "y") for n in (0, 1)]
+        rows // 2,
+    )
+    att2s, res2s = over_tp(att2), over_tp(res2)
+
+    gu_swp_my = pair(gu_swp_m, "y")
     dn_swp_m = swap(dn_swp, "zh")
     dn_swp_y = swap(dn_swp, "y")
     dn_own_my = swap(dn_own_m, "y")
     dn_swp_my = swap(dn_swp_m, "y")
 
-    pieces = [gu_own, gu_own_y, gu_swp, gu_swp_y, gu_own_m, gu_own_my]
+    pieces = [gu_own, gu_own_y, *gu_swp, *gu_swp_y, gu_own_m, gu_own_my]
     at = lambda n: 4 * (zh ^ (n // 4)) + 2 * (zl ^ (n // 2 % 2)) + (y ^ (n % 2))
     spots = jnp.stack([at(n) for n in range(8)]).astype(jnp.int32)
-    acts = partial_acts(spots[:6], normed, pieces, rows // 2)
-    hidden = hidden_units(
-        spots, normed, normed2, acts, [*pieces, *gu_swp_m, *gu_swp_my], 6, main, tail, rows // 2
-    )
+    last = [*gu_swp_m, *gu_swp_my]
+    where = jnp.concatenate([place, spots])
+    acts = near_step(
+        functools.partial(partial_kernel, len(pieces)), where, normed, (), pieces,
+        jax.ShapeDtypeStruct((rows, units), jnp.float32), PARTIAL_MIB, rows // 2,
+    )
+    near = near_step(
+        functools.partial(near_kernel, main, tail, len(last)), where, normed,
+        (acts,), last, jax.ShapeDtypeStruct((rows, main + tail), jnp.bfloat16), NEAR_MIB,
+        rows // 2,
+    )
+    pieces += last
+    far = far_hidden(where, att2s, outs, res2s, gains, pieces, main, tail, rows // 2)
 
     flags = jnp.stack([c == zl, x == zh]).astype(jnp.int32)
     wide = lambda v: v.astype(jnp.float32)
     add = lambda a, b: wide(a) + wide(b)
 
     def reduced(pieces, rows_first):
-        sent = down(flags, hidden, pieces, rows // 2)
+        sent = down(flags, near, far, pieces)
         got = swap(sent, "c")
-        total = down(flags, hidden, pieces, rows // 2, (got,))
+        total = down(flags, near, far, pieces, (got,))
         if rows_first:
             got = swap(total[rows:], "zl")
             total = add(total[:rows], got).astype(jnp.bfloat16)

time: 283 us -> 261 us (0.922)
  waiting for transfers between devices: 165 us -> 135 us
  starting transfers between devices: 38.3 us -> 48.1 us
    ppermute x42 -> x44, waiting for transfers between devices: 165 us -> 135 us  [swap(): return lax.ppermute(block, axis, [(0, 1), (1, 0)])]
    pallas_call x2 -> x3, Pallas kernels: 19.6 us -> 32.3 us  [the longest x1 17.3 us: far_hidden(): pl.pallas_call(functools.partial(far_kernel, main, tail, len(pieces)), gr...]
    ppermute x42 -> x44, starting transfers between devices: 33.4 us -> 44.7 us  [swap(): return lax.ppermute(block, axis, [(0, 1), (1, 0)])]
    pallas_call x2 -> x1, Pallas kernels: 19.7 us -> 10 us  [project(): pl.pallas_call(project_kernel, grid_spec=pltpu.PrefetchScalarGridSpec(num...]
    unnamed x56 -> x52, local copies, waits for them, and re-layouts: 7.42 us -> 5.27 us
  transfers between devices with their start and end apart: 43 -> 45, of which waited for: 18 -> 18; matrix products, arithmetic and copies ran while one was open for 2% -> 2% of each run, Pallas kernels for 21% -> 24%
where the time goes in v1:
time: 261 us
  waiting for transfers between devices  135 us (52%)
  Pallas kernels  66.7 us (26%)
  starting transfers between devices  48.1 us (18%)
  local copies, waits for them, and re-layouts  9.78 us (4%)
    ppermute x44, waiting for transfers between devices, swap(): return lax.ppermute(block, axis, [(0, 1), (1, 0)])  135 us
    ppermute x44, starting transfers between devices, swap(): return lax.ppermute(block, axis, [(0, 1), (1, 0)])  44.7 us
    pallas_call x1, Pallas kernels, far_hidden(): pl.pallas_call(functools.partial(far_kernel, main, tail, len(pieces)), gr...  17.3 us
    pallas_call x2, Pallas kernels, near_step(): pl.pallas_call(kernel, grid_spec=pltpu.PrefetchScalarGridSpec(num_scalar_...  15.1 us
    pallas_call x1, Pallas kernels, project(): pl.pallas_call(project_kernel, grid_spec=pltpu.PrefetchScalarGridSpec(num...  10 us
    pallas_call x4, Pallas kernels, down(): pl.pallas_call(functools.partial(down_kernel, bool(got)), grid_spec=pltpu...  8.83 us
    pallas_call x1, Pallas kernels, attend(): pl.pallas_call(attend_kernel, grid_spec=pltpu.PrefetchScalarGridSpec(num_...  8.31 us
    unnamed x52, local copies, waits for them, and re-layouts  5.27 us
  transfers between devices with their start and end apart: 45, of which 18 were waited for; matrix products, arithmetic and copies ran while one was open for 2% of the time, Pallas kernels for 24%

profile of v1, /device:TPU:0, one launch (start us, length us, event | category | flops | bytes accessed | tf_op | source)
XLA Modules:
  0.0 260.5 jit_solution(1347936974571839630)
XLA Ops:
  0.0 3.0 %collective-permute-start.10 = (f32[1,512]{1,0:T(1,128)}, f32[1,512]{1,0:T(1,128)S(1)}, u32[]{:S(2)}, u32[]{:S(2)}) collective-permute-start(f32[1,512]{1,0:T(1,128)} %bitcast.27), channel_id=1, source_target_pairs={{0,2},{2,0},{1,3},{3,1},{4,6},{6,4},{5,7},{7,5},{8,10},{10,8},{9,1... | collective-permute-start | bytes 6152 | tf_op jit(solution)/shard_map/ppermute | solution.py:116
  3.0 2.6 shard_map.119
  5.5 1.6 collective-permute-start.14
  8.6 3.4 %collective-permute-start = (bf16[128,128]{1,0:T(8,128)(2,1)S(1)}, bf16[128,128]{1,0:T(8,128)(2,1)S(1)}, u32[]{:S(2)}, u32[]{:S(2)}) collective-permute-start(bf16[128,128]{1,0:T(8,128)(2,1)S(1)} %pad_maximum_fusion), channel_id=1, source_target_pairs={{0,4},{4,8},{8,12},{12,16},{16,20},{20,24},{24,28},{1,5},{5,9},{9,... | collective-permute-start | bytes 98312 | tf_op jit(solution)/shard_map/ppermute | solution.py:20
  12.5 2.1 shard_map.122
  15.3 2.6 collective-permute-start.18
  17.9 1.6 collective-permute-start.32
  20.0 8.3 %attend.1.refs_0_ = bf16[768,256]{1,0:T(8,128)(2,1)} custom-call(s32[1]{0:T(128)} %bitcast.5.place_ref, f32[4]{0:T(128)} %sink_ref.1, bf16[768,256]{1,0:T(8,128)(2,1)} %q_ref.1, bf16[64,768]{1,0:T(8,128)(2,1)} %bitcast.23, bf16[64,768]{1,0:T(8,128)(2,1)} %bitcast.25, bf16[128,128]{1,0:T(8,128)(2,1)} %copy-done.22, f32[1,64]{1,0:T(1,128)} %bitcast.31, ...), custom_call_target="tpu_custom_call" | custom-call | flops 2516582400 | bytes 786432 | tf_op jit(solution)/shard_map/attend/pallas_call | solution.py:179
  28.4 0.9 collective-permute-start.24
  29.3 9.6 %collective-permute-start.33 = (bf16[704,256]{1,0:T(8,128)(2,1)S(1)}, bf16[704,256]{1,0:T(8,128)(2,1)S(1)}, u32[]{:S(2)}, u32[]{:S(2)}) collective-permute-start(bf16[704,256]{1,0:T(8,128)(2,1)S(1)} %copy-done.2), channel_id=1, source_target_pairs={{0,16},{16,0},{1,17},{17,1},{2,18},{18,2},{3,19},{19,3},{4,20},{20... | collective-permute-start | bytes 1081352 | tf_op jit(solution)/shard_map/ppermute | solution.py:116
  39.4 7.8 %collective-permute-done.32.refs_1_ = bf16[704,256]{1,0:T(8,128)(2,1)S(1)} collective-permute-done((bf16[704,256]{1,0:T(8,128)(2,1)}, bf16[704,256]{1,0:T(8,128)(2,1)S(1)}, u32[]{:S(2)}, u32[]{:S(2)}) %collective-permute-start.32) | collective-permute-done | bytes 360480 | tf_op jit(solution)/shard_map/ppermute | solution.py:116
  47.2 15.6 %collective-permute-done.33.refs_2_ = bf16[704,256]{1,0:T(8,128)(2,1)S(1)} collective-permute-done((bf16[704,256]{1,0:T(8,128)(2,1)S(1)}, bf16[704,256]{1,0:T(8,128)(2,1)S(1)}, u32[]{:S(2)}, u32[]{:S(2)}) %collective-permute-start.33) | collective-permute-done | bytes 360480 | tf_op jit(solution)/shard_map/ppermute | solution.py:116
  62.8 3.4 %collective-permute-start.20 = (bf16[128,1408]{1,0:T(8,128)(2,1)S(1)}, bf16[128,1408]{1,0:T(8,128)(2,1)S(1)}, u32[]{:S(2)}, u32[]{:S(2)}) collective-permute-start(bf16[128,1408]{1,0:T(8,128)(2,1)S(1)} %collective-permute-done.14.refs_2_.refs_18_), channel_id=1, source_target_pairs={{0,16},{16,0},{1,17},{17,1},{2,18},{18,2},{3,19},{19,3},{4,20},{20... | collective-permute-start | bytes 1081352 | tf_op jit(solution)/shard_map/ppermute | solution.py:116
  66.9 4.3 %collective-permute-start.16 = (bf16[128,1408]{1,0:T(8,128)(2,1)S(1)}, bf16[128,1408]{1,0:T(8,128)(2,1)S(1)}, u32[]{:S(2)}, u32[]{:S(2)}) collective-permute-start(bf16[128,1408]{1,0:T(8,128)(2,1)S(1)} %collective-permute-done.14.refs_2_.refs_18_), channel_id=1, source_target_pairs={{0,4},{4,0},{1,5},{5,1},{2,6},{6,2},{3,7},{7,3},{8,12},{12,8},{9,1... | collective-permute-start | bytes 1081352 | tf_op jit(solution)/shard_map/ppermute | solution.py:116
  71.3 19.6 %collective-permute-done.20.refs_0_.refs_24_ = bf16[128,1408]{1,0:T(8,128)(2,1)S(1)} collective-permute-done((bf16[128,1408]{1,0:T(8,128)(2,1)S(1)}, bf16[128,1408]{1,0:T(8,128)(2,1)S(1)}, u32[]{:S(2)}, u32[]{:S(2)}) %collective-permute-start.20) | collective-permute-done | bytes 360480 | tf_op jit(solution)/shard_map/ppermute | solution.py:116
  91.0 6.7 %collective-permute-done.21.refs_1_.refs_25_ = bf16[128,1408]{1,0:T(8,128)(2,1)S(1)} collective-permute-done((bf16[128,1408]{1,0:T(8,128)(2,1)}, bf16[128,1408]{1,0:T(8,128)(2,1)S(1)}, u32[]{:S(2)}, u32[]{:S(2)}) %collective-permute-start.21) | collective-permute-done | bytes 360480 | tf_op jit(solution)/shard_map/ppermute | solution.py:116
  97.7 2.2 collective-permute-start.13
  101.1 13.8 %collective-permute-done.13.refs_1_.refs_17_ = bf16[256,1408]{1,0:T(8,128)(2,1)S(1)} collective-permute-done((bf16[256,1408]{1,0:T(8,128)(2,1)}, bf16[256,1408]{1,0:T(8,128)(2,1)S(1)}, u32[]{:S(2)}, u32[]{:S(2)}) %collective-permute-start.13) | collective-permute-done | bytes 720928 | tf_op jit(solution)/shard_map/ppermute | solution.py:116
  116.0 3.9 %collective-permute-done.7.refs_9_ = bf16[768,512]{1,0:T(8,128)(2,1)} collective-permute-done((bf16[768,512]{1,0:T(8,128)(2,1)}, bf16[768,512]{1,0:T(8,128)(2,1)}, u32[]{:S(2)}, u32[]{:S(2)}) %collective-permute-start.7) | collective-permute-done | bytes 786464 | tf_op jit(solution)/shard_map/ppermute | solution.py:116
  120.4 7.8 %collective-permute-done.25.refs_1_ = bf16[768,256]{1,0:T(8,128)(2,1)S(1)} collective-permute-done((bf16[768,256]{1,0:T(8,128)(2,1)S(1)}, bf16[768,256]{1,0:T(8,128)(2,1)S(1)}, u32[]{:S(2)}, u32[]{:S(2)}) %collective-permute-start.25) | collective-permute-done | bytes 393248 | tf_op jit(solution)/shard_map/ppermute | solution.py:116
  128.2 0.8 copy-done.14
  129.0 1.7 collective-permute-done.3.refs_3_
  130.7 0.7 copy-done.17
  131.8 1.7 collective-permute-start.22
  133.6 9.5 %collective-permute-done.29.refs_9_ = bf16[768,512]{1,0:T(8,128)(2,1)} collective-permute-done((bf16[768,512]{1,0:T(8,128)(2,1)}, bf16[768,512]{1,0:T(8,128)(2,1)}, u32[]{:S(2)}, u32[]{:S(2)}) %collective-permute-start.29) | collective-permute-done | bytes 786464 | tf_op jit(solution)/shard_map/ppermute | solution.py:116
  145.2 10.0 %shard_map.118 = (bf16[768,2048]{1,0:T(8,128)(2,1)}, bf16[768,512]{1,0:T(8,128)(2,1)}) custom-call(s32[4]{0:T(128)} %pad_add_fusion.place_ref, bf16[768,256]{1,0:T(8,128)(2,1)} %attend.1.refs_0_, bf16[768,256]{1,0:T(8,128)(2,1)} %copy-done.15, bf16[768,256]{1,0:T(8,128)(2,1)} %copy-done.16, bf16[768,256]{1,0:T(8,128)(2,1)} %copy-done.17, ...), custom_call_target="tpu_custom_call" | custom-call | flops 3221225472 | bytes 6291456 | tf_op jit(solution)/shard_map/pallas_call | solution.py:283
  155.2 3.2 %collective-permute-done.22.refs_2_.refs_26_ = bf16[128,1408]{1,0:T(8,128)(2,1)S(1)} collective-permute-done((bf16[128,1408]{1,0:T(8,128)(2,1)S(1)}, bf16[128,1408]{1,0:T(8,128)(2,1)S(1)}, u32[]{:S(2)}, u32[]{:S(2)}) %collective-permute-start.22) | collective-permute-done | bytes 360480 | tf_op jit(solution)/shard_map/ppermute | solution.py:116
  158.4 6.9 %collective-permute-done.23.refs_3_.refs_27_ = bf16[128,1408]{1,0:T(8,128)(2,1)S(1)} collective-permute-done((bf16[128,1408]{1,0:T(8,128)(2,1)S(1)}, bf16[128,1408]{1,0:T(8,128)(2,1)S(1)}, u32[]{:S(2)}, u32[]{:S(2)}) %collective-permute-start.23) | collective-permute-done | bytes 360480 | tf_op jit(solution)/shard_map/ppermute | solution.py:116
  165.8 9.1 %shard_map.120.acts_ref = f32[768,1408]{1,0:T(8,128)} custom-call(s32[12]{0:T(128)} %concatenate.8.place_ref, bf16[768,2048]{1,0:T(8,128)(2,1)} %get-tuple-element.13.x_ref, bf16[256,1408]{1,0:T(8,128)(2,1)} %get-tuple-element.14.refs_0_.refs_16_, bf16[256,1408]{1,0:T(8,128)(2,1)} %copy-done.12, bf16[128,1408]{1,0:T(8,128)(2,1)} %copy-done.18, ...), custom_call_target="tpu_custom_call" | custom-call | flops 3538944000 | bytes 3072000 | tf_op jit(solution)/shard_map/pallas_call | solution.py:391
  174.9 6.0 %shard_map.121.near_ref = bf16[768,704]{1,0:T(8,128)(2,1)} custom-call(s32[12]{0:T(128)} %concatenate.8.place_ref, bf16[768,2048]{1,0:T(8,128)(2,1)} %get-tuple-element.13.x_ref, f32[768,1408]{1,0:T(8,128)} %shard_map.120.acts_ref, bf16[128,1408]{1,0:T(8,128)(2,1)} %copy-done.5, bf16[128,1408]{1,0:T(8,128)(2,1)} %copy-done.6, bf16[128,1408]{1,0:T(8,128)(2,1)} %copy-done.7, ...), custom_call_target="tpu_custom_call" | custom-call | flops 1179648000 | bytes 3072000 | tf_op jit(solution)/shard_map/pallas_call | solution.py:391
  181.3 1.7 collective-permute-start.39
  183.3 1.7 collective-permute-start.41
  185.0 17.3 %far_hidden.1.far_ref = bf16[768,704]{1,0:T(8,128)(2,1)} custom-call(s32[12]{0:T(128)} %concatenate.8.place_ref, bf16[768,256]{1,0:T(8,128)(2,1)} %copy-done.13, bf16[768,256]{1,0:T(8,128)(2,1)} %copy-done.14, bf16[768,256]{1,0:T(8,128)(2,1)} %collective-permute-done.26.refs_2_, bf16[768,256]{1,0:T(8,128)(2,1)} %collective-permute-done.27.refs_3_, ...), custom_call_target="tpu_custom_call" | custom-call | flops 8858370048 | bytes 8650752 | tf_op jit(solution)/shard_map/far_hidden/pallas_call | solution.py:347
  202.3 5.4 %collective-permute-done.40.refs_2_ = bf16[704,256]{1,0:T(8,128)(2,1)S(1)} collective-permute-done((bf16[704,256]{1,0:T(8,128)(2,1)S(1)}, bf16[704,256]{1,0:T(8,128)(2,1)S(1)}, u32[]{:S(2)}, u32[]{:S(2)}) %collective-permute-start.40) | collective-permute-done | bytes 360480 | tf_op jit(solution)/shard_map/ppermute | solution.py:116
  207.7 6.8 %collective-permute-done.41.refs_3_ = bf16[704,256]{1,0:T(8,128)(2,1)S(1)} collective-permute-done((bf16[704,256]{1,0:T(8,128)(2,1)S(1)}, bf16[704,256]{1,0:T(8,128)(2,1)S(1)}, u32[]{:S(2)}, u32[]{:S(2)}) %collective-permute-start.41) | collective-permute-done | bytes 360480 | tf_op jit(solution)/shard_map/ppermute | solution.py:116
  214.5 1.3 copy-done.1
  215.8 2.2 shard_map.125
  218.1 2.2 shard_map.123
  221.5 2.2 shard_map.126
  224.4 2.2 shard_map.124
  227.2 16.2 %collective-permute-done.43 = bf16[1536,256]{1,0:T(8,128)(2,1)S(1)} collective-permute-done((bf16[1536,256]{1,0:T(8,128)(2,1)S(1)}, bf16[1536,256]{1,0:T(8,128)(2,1)S(1)}, u32[]{:S(2)}, u32[]{:S(2)}) %collective-permute-start.43) | collective-permute-done | bytes 786464 | tf_op jit(solution)/shard_map/ppermute | solution.py:116
  243.6 0.8 fusion
  245.0 1.1 collective-permute-done.36
  246.3 0.8 fusion.1
  247.1 2.1 collective-permute-start.37
  249.2 5.6 %collective-permute-done.44.behind_got = bf16[768,256]{1,0:T(8,128)(2,1)S(1)} collective-permute-done((bf16[768,256]{1,0:T(8,128)(2,1)S(1)}, bf16[768,256]{1,0:T(8,128)(2,1)S(1)}, u32[]{:S(2)}, u32[]{:S(2)}) %collective-permute-start.44) | collective-permute-done | bytes 393248 | tf_op jit(solution)/shard_map/ppermute | solution.py:116
  254.7 2.4 collective-permute-done.37.ahead_got
  257.9 2.6 finish.1
  (119 shorter events, 15.5 us)
Async XLA Ops:
  0.0 15.3 %collective-permute-start.10 = (f32[1,512]{1,0:T(1,128)}, f32[1,512]{1,0:T(1,128)S(1)}, u32[]{:S(2)}, u32[]{:S(2)}) collective-permute-start(f32[1,512]{1,0:T(1,128)} %bitcast.27), channel_id=1, source_target_pairs={{0,2},{2,0},{1,3},{3,1},{4,6},{6,4},{5,7},{7,5},{8,10},{10,8},{9,1... | collective-permute-start | bytes 6152 | tf_op jit(solution)/shard_map/ppermute | solution.py:116
  3.0 14.9 %collective-permute-start.11 = (f32[1,512]{1,0:T(1,128)}, f32[1,512]{1,0:T(1,128)S(1)}, u32[]{:S(2)}, u32[]{:S(2)}) collective-permute-start(f32[1,512]{1,0:T(1,128)} %bitcast.28), channel_id=1, source_target_pairs={{0,1},{1,0},{2,3},{3,2},{4,5},{5,4},{6,7},{7,6},{8,9},{9,8},{10,11... | collective-permute-start | bytes 6152 | tf_op jit(solution)/shard_map/ppermute | solution.py:116
  5.5 23.7 %collective-permute-start.14 = (bf16[128,1408]{1,0:T(8,128)(2,1)}, bf16[128,1408]{1,0:T(8,128)(2,1)S(1)}, u32[]{:S(2)}, u32[]{:S(2)}) collective-permute-start(bf16[128,1408]{1,0:T(8,128)(2,1)} %get-tuple-element.15), channel_id=1, source_target_pairs={{0,8},{8,0},{1,9},{9,1},{2,10},{10,2},{3,11},{11,3},{4,12},{12,4},... | collective-permute-start | bytes 1081352 | tf_op jit(solution)/shard_map/ppermute | solution.py:116
  8.6 10.9 %collective-permute-start = (bf16[128,128]{1,0:T(8,128)(2,1)S(1)}, bf16[128,128]{1,0:T(8,128)(2,1)S(1)}, u32[]{:S(2)}, u32[]{:S(2)}) collective-permute-start(bf16[128,128]{1,0:T(8,128)(2,1)S(1)} %pad_maximum_fusion), channel_id=1, source_target_pairs={{0,4},{4,8},{8,12},{12,16},{16,20},{20,24},{24,28},{1,5},{5,9},{9,... | collective-permute-start | bytes 98312 | tf_op jit(solution)/shard_map/ppermute | solution.py:20
  12.0 26.9 %collective-permute-start.15 = (bf16[128,1408]{1,0:T(8,128)(2,1)}, bf16[128,1408]{1,0:T(8,128)(2,1)S(1)}, u32[]{:S(2)}, u32[]{:S(2)}) collective-permute-start(bf16[128,1408]{1,0:T(8,128)(2,1)} %get-tuple-element.16), channel_id=1, source_target_pairs={{0,8},{8,0},{1,9},{9,1},{2,10},{10,2},{3,11},{11,3},{4,12},{12,4},... | collective-permute-start | bytes 1081352 | tf_op jit(solution)/shard_map/ppermute | solution.py:116
  15.3 56.0 %collective-permute-start.18 = (bf16[256,1408]{1,0:T(8,128)(2,1)}, bf16[256,1408]{1,0:T(8,128)(2,1)}, u32[]{:S(2)}, u32[]{:S(2)}) collective-permute-start(bf16[256,1408]{1,0:T(8,128)(2,1)} %get-tuple-element.14.refs_0_.refs_16_), channel_id=1, source_target_pairs={{0,16},{16,0},{1,17},{17,1},{2,18},{18,2},{3,19},{19,3},{4,20},{20... | collective-permute-start | bytes 2162696 | tf_op jit(solution)/shard_map/ppermute | solution.py:116
  17.9 29.3 %collective-permute-start.32 = (bf16[704,256]{1,0:T(8,128)(2,1)}, bf16[704,256]{1,0:T(8,128)(2,1)S(1)}, u32[]{:S(2)}, u32[]{:S(2)}) collective-permute-start(bf16[704,256]{1,0:T(8,128)(2,1)} %get-tuple-element.18), channel_id=1, source_target_pairs={{0,8},{8,0},{1,9},{9,1},{2,10},{10,2},{3,11},{11,3},{4,12},{12,4},... | collective-permute-start | bytes 1081352 | tf_op jit(solution)/shard_map/ppermute | solution.py:116
  19.4 8.9 %collective-permute-start.12 = (f32[1,512]{1,0:T(1,128)S(1)}, f32[1,512]{1,0:T(1,128)S(1)}, u32[]{:S(2)}, u32[]{:S(2)}) collective-permute-start(f32[1,512]{1,0:T(1,128)S(1)} %collective-permute-done.10.refs_13_), channel_id=1, source_target_pairs={{0,1},{1,0},{2,3},{3,2},{4,5},{5,4},{6,7},{7,6},{8,9},{9,8},{10,11... | collective-permute-start | bytes 6152 | tf_op jit(solution)/shard_map/ppermute | solution.py:116
  28.4 116.8 %copy-start.25 = (f32[1,512]{1,0:T(1,128)}, f32[1,512]{1,0:T(1,128)S(1)}, u32[]{:S(2)}) copy-start(f32[1,512]{1,0:T(1,128)S(1)} %collective-permute-done.12.refs_15_) | copy-start | bytes 6148
  28.4 37.9 %collective-permute-start.24 = (bf16[768,256]{1,0:T(8,128)(2,1)}, bf16[768,256]{1,0:T(8,128)(2,1)S(1)}, u32[]{:S(2)}, u32[]{:S(2)}) collective-permute-start(bf16[768,256]{1,0:T(8,128)(2,1)} %attend.1.refs_0_), channel_id=1, source_target_pairs={{0,8},{8,0},{1,9},{9,1},{2,10},{10,2},{3,11},{11,3},{4,12},{12,4},... | collective-permute-start | bytes 1179656 | tf_op jit(solution)/shard_map/ppermute | solution.py:116
  29.3 102.6 %copy-start.18 = (bf16[128,1408]{1,0:T(8,128)(2,1)}, bf16[128,1408]{1,0:T(8,128)(2,1)S(1)}, u32[]{:S(2)}) copy-start(bf16[128,1408]{1,0:T(8,128)(2,1)S(1)} %collective-permute-done.14.refs_2_.refs_18_) | copy-start | bytes 1081348
  29.3 33.5 %collective-permute-start.33 = (bf16[704,256]{1,0:T(8,128)(2,1)S(1)}, bf16[704,256]{1,0:T(8,128)(2,1)S(1)}, u32[]{:S(2)}, u32[]{:S(2)}) collective-permute-start(bf16[704,256]{1,0:T(8,128)(2,1)S(1)} %copy-done.2), channel_id=1, source_target_pairs={{0,16},{16,0},{1,17},{17,1},{2,18},{18,2},{3,19},{19,3},{4,20},{20... | collective-permute-start | bytes 1081352 | tf_op jit(solution)/shard_map/ppermute | solution.py:116
  38.9 27.5 %collective-permute-start.1 = (bf16[768,256]{1,0:T(8,128)(2,1)}, bf16[768,256]{1,0:T(8,128)(2,1)S(1)}, u32[]{:S(2)}, u32[]{:S(2)}) collective-permute-start(bf16[768,256]{1,0:T(8,128)(2,1)} %attend.1.refs_0_), channel_id=1, source_target_pairs={{0,2},{2,0},{1,3},{3,1},{4,6},{6,4},{5,7},{7,5},{8,10},{10,8},{9,1... | collective-permute-start | bytes 1179656 | tf_op jit(solution)/shard_map/ppermute | solution.py:116
  47.2 19.7 %collective-permute-start.2 = (bf16[768,256]{1,0:T(8,128)(2,1)}, bf16[768,256]{1,0:T(8,128)(2,1)S(1)}, u32[]{:S(2)}, u32[]{:S(2)}) collective-permute-start(bf16[768,256]{1,0:T(8,128)(2,1)} %attend.1.refs_0_), channel_id=1, source_target_pairs={{0,1},{1,0},{2,3},{3,2},{4,5},{5,4},{6,7},{7,6},{8,9},{9,8},{10,11... | collective-permute-start | bytes 1179656 | tf_op jit(solution)/shard_map/ppermute | solution.py:116
  62.8 28.1 %collective-permute-start.20 = (bf16[128,1408]{1,0:T(8,128)(2,1)S(1)}, bf16[128,1408]{1,0:T(8,128)(2,1)S(1)}, u32[]{:S(2)}, u32[]{:S(2)}) collective-permute-start(bf16[128,1408]{1,0:T(8,128)(2,1)S(1)} %collective-permute-done.14.refs_2_.refs_18_), channel_id=1, source_target_pairs={{0,16},{16,0},{1,17},{17,1},{2,18},{18,2},{3,19},{19,3},{4,20},{20... | collective-permute-start | bytes 1081352 | tf_op jit(solution)/shard_map/ppermute | solution.py:116
  66.2 31.4 %collective-permute-start.21 = (bf16[128,1408]{1,0:T(8,128)(2,1)}, bf16[128,1408]{1,0:T(8,128)(2,1)S(1)}, u32[]{:S(2)}, u32[]{:S(2)}) collective-permute-start(bf16[128,1408]{1,0:T(8,128)(2,1)} %copy-done.19), channel_id=1, source_target_pairs={{0,16},{16,0},{1,17},{17,1},{2,18},{18,2},{3,19},{19,3},{4,20},{20... | collective-permute-start | bytes 1081352 | tf_op jit(solution)/shard_map/ppermute | solution.py:116
  66.3 49.1 %collective-permute-start.4 = (bf16[256,2048]{1,0:T(8,128)(2,1)S(1)}, bf16[256,2048]{1,0:T(8,128)(2,1)}, u32[]{:S(2)}, u32[]{:S(2)}) collective-permute-start(bf16[256,2048]{1,0:T(8,128)(2,1)S(1)} %copy-done.10), channel_id=1, source_target_pairs={{0,2},{2,0},{1,3},{3,1},{4,6},{6,4},{5,7},{7,5},{8,10},{10,8},{9,1... | collective-permute-start | bytes 3145736 | tf_op jit(solution)/shard_map/ppermute | solution.py:116
  66.9 32.9 %collective-permute-start.16 = (bf16[128,1408]{1,0:T(8,128)(2,1)S(1)}, bf16[128,1408]{1,0:T(8,128)(2,1)S(1)}, u32[]{:S(2)}, u32[]{:S(2)}) collective-permute-start(bf16[128,1408]{1,0:T(8,128)(2,1)S(1)} %collective-permute-done.14.refs_2_.refs_18_), channel_id=1, source_target_pairs={{0,4},{4,0},{1,5},{5,1},{2,6},{6,2},{3,7},{7,3},{8,12},{12,8},{9,1... | collective-permute-start | bytes 1081352 | tf_op jit(solution)/shard_map/ppermute | solution.py:116
  71.3 29.1 %collective-permute-start.17 = (bf16[128,1408]{1,0:T(8,128)(2,1)}, bf16[128,1408]{1,0:T(8,128)(2,1)S(1)}, u32[]{:S(2)}, u32[]{:S(2)}) collective-permute-start(bf16[128,1408]{1,0:T(8,128)(2,1)} %copy-done.19), channel_id=1, source_target_pairs={{0,4},{4,0},{1,5},{5,1},{2,6},{6,2},{3,7},{7,3},{8,12},{12,8},{9,1... | collective-permute-start | bytes 1081352 | tf_op jit(solution)/shard_map/ppermute | solution.py:116
  90.9 64.2 %copy-start.5 = (bf16[128,1408]{1,0:T(8,128)(2,1)}, bf16[128,1408]{1,0:T(8,128)(2,1)S(1)}, u32[]{:S(2)}) copy-start(bf16[128,1408]{1,0:T(8,128)(2,1)S(1)} %collective-permute-done.20.refs_0_.refs_24_) | copy-start | bytes 1081348
  90.9 24.5 %collective-permute-start.28 = (bf16[768,512]{1,0:T(8,128)(2,1)}, bf16[768,512]{1,0:T(8,128)(2,1)}, u32[]{:S(2)}, u32[]{:S(2)}) collective-permute-start(bf16[768,512]{1,0:T(8,128)(2,1)} %refs_8_.1), channel_id=1, source_target_pairs={{0,8},{8,0},{1,9},{9,1},{2,10},{10,2},{3,11},{11,3},{4,12},{12,4},... | collective-permute-start | bytes 2359304 | tf_op jit(solution)/shard_map/ppermute | solution.py:116
  97.7 17.2 %collective-permute-start.13 = (bf16[256,1408]{1,0:T(8,128)(2,1)}, bf16[256,1408]{1,0:T(8,128)(2,1)S(1)}, u32[]{:S(2)}, u32[]{:S(2)}) collective-permute-start(bf16[256,1408]{1,0:T(8,128)(2,1)} %get-tuple-element.14.refs_0_.refs_16_), channel_id=1, source_target_pairs={{0,4},{4,0},{1,5},{5,1},{2,6},{6,2},{3,7},{7,3},{8,12},{12,8},{9,1... | collective-permute-start | bytes 2162696 | tf_op jit(solution)/shard_map/ppermute | solution.py:116
  99.9 20.0 %collective-permute-start.7 = (bf16[768,512]{1,0:T(8,128)(2,1)}, bf16[768,512]{1,0:T(8,128)(2,1)}, u32[]{:S(2)}, u32[]{:S(2)}) collective-permute-start(bf16[768,512]{1,0:T(8,128)(2,1)} %refs_8_.1), channel_id=1, source_target_pairs={{0,2},{2,0},{1,3},{3,1},{4,6},{6,4},{5,7},{7,5},{8,10},{10,8},{9,1... | collective-permute-start | bytes 2359304 | tf_op jit(solution)/shard_map/ppermute | solution.py:116
  100.4 20.0 %collective-permute-start.8 = (bf16[768,512]{1,0:T(8,128)(2,1)}, bf16[768,512]{1,0:T(8,128)(2,1)}, u32[]{:S(2)}, u32[]{:S(2)}) collective-permute-start(bf16[768,512]{1,0:T(8,128)(2,1)} %refs_8_.1), channel_id=1, source_target_pairs={{0,1},{1,0},{2,3},{3,2},{4,5},{5,4},{6,7},{7,6},{8,9},{9,8},{10,11... | collective-permute-start | bytes 2359304 | tf_op jit(solution)/shard_map/ppermute | solution.py:116
  114.9 13.3 %collective-permute-start.25 = (bf16[768,256]{1,0:T(8,128)(2,1)S(1)}, bf16[768,256]{1,0:T(8,128)(2,1)S(1)}, u32[]{:S(2)}, u32[]{:S(2)}) collective-permute-start(bf16[768,256]{1,0:T(8,128)(2,1)S(1)} %collective-permute-done.24.refs_0_), channel_id=1, source_target_pairs={{0,2},{2,0},{1,3},{3,1},{4,6},{6,4},{5,7},{7,5},{8,10},{10,8},{9,1... | collective-permute-start | bytes 1179656 | tf_op jit(solution)/shard_map/ppermute | solution.py:116
  115.4 16.4 %collective-permute-start.5 = (bf16[256,2048]{1,0:T(8,128)(2,1)S(1)}, bf16[256,2048]{1,0:T(8,128)(2,1)}, u32[]{:S(2)}, u32[]{:S(2)}) collective-permute-start(bf16[256,2048]{1,0:T(8,128)(2,1)S(1)} %copy-done.10), channel_id=1, source_target_pairs={{0,1},{1,0},{2,3},{3,2},{4,5},{5,4},{6,7},{7,6},{8,9},{9,8},{10,11... | collective-permute-start | bytes 3145736 | tf_op jit(solution)/shard_map/ppermute | solution.py:116
  115.8 27.7 %collective-permute-start.6 = (bf16[256,2048]{1,0:T(8,128)(2,1)}, bf16[256,2048]{1,0:T(8,128)(2,1)}, u32[]{:S(2)}, u32[]{:S(2)}) collective-permute-start(bf16[256,2048]{1,0:T(8,128)(2,1)} %collective-permute-done.4.refs_5_), channel_id=1, source_target_pairs={{0,1},{1,0},{2,3},{3,2},{4,5},{5,4},{6,7},{7,6},{8,9},{9,8},{10,11... | collective-permute-start | bytes 3145736 | tf_op jit(solution)/shard_map/ppermute | solution.py:116
  119.9 23.2 %collective-permute-start.29 = (bf16[768,512]{1,0:T(8,128)(2,1)}, bf16[768,512]{1,0:T(8,128)(2,1)}, u32[]{:S(2)}, u32[]{:S(2)}) collective-permute-start(bf16[768,512]{1,0:T(8,128)(2,1)} %collective-permute-done.28.refs_8_), channel_id=1, source_target_pairs={{0,2},{2,0},{1,3},{3,1},{4,6},{6,4},{5,7},{7,5},{8,10},{10,8},{9,1... | collective-permute-start | bytes 2359304 | tf_op jit(solution)/shard_map/ppermute | solution.py:116
  120.4 23.0 %collective-permute-start.9 = (bf16[768,512]{1,0:T(8,128)(2,1)}, bf16[768,512]{1,0:T(8,128)(2,1)}, u32[]{:S(2)}, u32[]{:S(2)}) collective-permute-start(bf16[768,512]{1,0:T(8,128)(2,1)} %collective-permute-done.7.refs_9_), channel_id=1, source_target_pairs={{0,1},{1,0},{2,3},{3,2},{4,5},{5,4},{6,7},{7,6},{8,9},{9,8},{10,11... | collective-permute-start | bytes 2359304 | tf_op jit(solution)/shard_map/ppermute | solution.py:116
  129.0 1.7 collective-permute-start.3
  131.4 33.8 %collective-permute-start.19 = (bf16[256,1408]{1,0:T(8,128)(2,1)}, bf16[256,1408]{1,0:T(8,128)(2,1)}, u32[]{:S(2)}, u32[]{:S(2)}) collective-permute-start(bf16[256,1408]{1,0:T(8,128)(2,1)} %collective-permute-done.18.refs_6_.refs_22_), channel_id=1, source_target_pairs={{0,4},{4,0},{1,5},{5,1},{2,6},{6,2},{3,7},{7,3},{8,12},{12,8},{9,1... | collective-permute-start | bytes 2162696 | tf_op jit(solution)/shard_map/ppermute | solution.py:116
  131.8 26.5 %collective-permute-start.22 = (bf16[128,1408]{1,0:T(8,128)(2,1)S(1)}, bf16[128,1408]{1,0:T(8,128)(2,1)S(1)}, u32[]{:S(2)}, u32[]{:S(2)}) collective-permute-start(bf16[128,1408]{1,0:T(8,128)(2,1)S(1)} %collective-permute-done.20.refs_0_.refs_24_), channel_id=1, source_target_pairs={{0,4},{4,0},{1,5},{5,1},{2,6},{6,2},{3,7},{7,3},{8,12},{12,8},{9,1... | collective-permute-start | bytes 1081352 | tf_op jit(solution)/shard_map/ppermute | solution.py:116
  143.0 22.2 %collective-permute-start.23 = (bf16[128,1408]{1,0:T(8,128)(2,1)S(1)}, bf16[128,1408]{1,0:T(8,128)(2,1)S(1)}, u32[]{:S(2)}, u32[]{:S(2)}) collective-permute-start(bf16[128,1408]{1,0:T(8,128)(2,1)S(1)} %collective-permute-done.21.refs_1_.refs_25_), channel_id=1, source_target_pairs={{0,4},{4,0},{1,5},{5,1},{2,6},{6,2},{3,7},{7,3},{8,12},{12,8},{9,1... | collective-permute-start | bytes 1081352 | tf_op jit(solution)/shard_map/ppermute | solution.py:116
  143.4 39.9 %collective-permute-start.30 = (bf16[768,512]{1,0:T(8,128)(2,1)}, bf16[768,512]{1,0:T(8,128)(2,1)S(1)}, u32[]{:S(2)}, u32[]{:S(2)}) collective-permute-start(bf16[768,512]{1,0:T(8,128)(2,1)} %collective-permute-done.28.refs_8_), channel_id=1, source_target_pairs={{0,1},{1,0},{2,3},{3,2},{4,5},{5,4},{6,7},{7,6},{8,9},{9,8},{10,11... | collective-permute-start | bytes 2359304 | tf_op jit(solution)/shard_map/ppermute | solution.py:116
  143.4 41.6 %collective-permute-start.31 = (bf16[768,512]{1,0:T(8,128)(2,1)}, bf16[768,512]{1,0:T(8,128)(2,1)}, u32[]{:S(2)}, u32[]{:S(2)}) collective-permute-start(bf16[768,512]{1,0:T(8,128)(2,1)} %collective-permute-done.29.refs_9_), channel_id=1, source_target_pairs={{0,1},{1,0},{2,3},{3,2},{4,5},{5,4},{6,7},{7,6},{8,9},{9,8},{10,11... | collective-permute-start | bytes 2359304 | tf_op jit(solution)/shard_map/ppermute | solution.py:116
  158.4 22.5 %collective-permute-start.34 = (bf16[704,256]{1,0:T(8,128)(2,1)S(1)}, bf16[704,256]{1,0:T(8,128)(2,1)S(1)}, u32[]{:S(2)}, u32[]{:S(2)}) collective-permute-start(bf16[704,256]{1,0:T(8,128)(2,1)S(1)} %collective-permute-done.32.refs_1_), channel_id=1, source_target_pairs={{0,16},{16,0},{1,17},{17,1},{2,18},{18,2},{3,19},{19,3},{4,20},{20... | collective-permute-start | bytes 1081352 | tf_op jit(solution)/shard_map/ppermute | solution.py:116
  165.3 16.0 %collective-permute-start.26 = (bf16[768,256]{1,0:T(8,128)(2,1)}, bf16[768,256]{1,0:T(8,128)(2,1)}, u32[]{:S(2)}, u32[]{:S(2)}) collective-permute-start(bf16[768,256]{1,0:T(8,128)(2,1)} %copy-done.13), channel_id=1, source_target_pairs={{0,1},{1,0},{2,3},{3,2},{4,5},{5,4},{6,7},{7,6},{8,9},{9,8},{10,11... | collective-permute-start | bytes 1179656 | tf_op jit(solution)/shard_map/ppermute | solution.py:116
  165.3 17.7 %collective-permute-start.27 = (bf16[768,256]{1,0:T(8,128)(2,1)}, bf16[768,256]{1,0:T(8,128)(2,1)}, u32[]{:S(2)}, u32[]{:S(2)}) collective-permute-start(bf16[768,256]{1,0:T(8,128)(2,1)} %copy-done.14), channel_id=1, source_target_pairs={{0,1},{1,0},{2,3},{3,2},{4,5},{5,4},{6,7},{7,6},{8,9},{9,8},{10,11... | collective-permute-start | bytes 1179656 | tf_op jit(solution)/shard_map/ppermute | solution.py:116
  180.9 21.4 %collective-permute-start.38 = (bf16[704,256]{1,0:T(8,128)(2,1)S(1)}, bf16[704,256]{1,0:T(8,128)(2,1)S(1)}, u32[]{:S(2)}, u32[]{:S(2)}) collective-permute-start(bf16[704,256]{1,0:T(8,128)(2,1)S(1)} %copy-done.2), channel_id=1, source_target_pairs={{0,4},{4,0},{1,5},{5,1},{2,6},{6,2},{3,7},{7,3},{8,12},{12,8},{9,1... | collective-permute-start | bytes 1081352 | tf_op jit(solution)/shard_map/ppermute | solution.py:116
  181.3 26.4 %collective-permute-start.39 = (bf16[704,256]{1,0:T(8,128)(2,1)S(1)}, bf16[704,256]{1,0:T(8,128)(2,1)S(1)}, u32[]{:S(2)}, u32[]{:S(2)}) collective-permute-start(bf16[704,256]{1,0:T(8,128)(2,1)S(1)} %collective-permute-done.32.refs_1_), channel_id=1, source_target_pairs={{0,4},{4,0},{1,5},{5,1},{2,6},{6,2},{3,7},{7,3},{8,12},{12,8},{9,1... | collective-permute-start | bytes 1081352 | tf_op jit(solution)/shard_map/ppermute | solution.py:116
  183.0 24.7 %collective-permute-start.40 = (bf16[704,256]{1,0:T(8,128)(2,1)S(1)}, bf16[704,256]{1,0:T(8,128)(2,1)S(1)}, u32[]{:S(2)}, u32[]{:S(2)}) collective-permute-start(bf16[704,256]{1,0:T(8,128)(2,1)S(1)} %collective-permute-done.33.refs_2_), channel_id=1, source_target_pairs={{0,4},{4,0},{1,5},{5,1},{2,6},{6,2},{3,7},{7,3},{8,12},{12,8},{9,1... | collective-permute-start | bytes 1081352 | tf_op jit(solution)/shard_map/ppermute | solution.py:116
  183.3 31.2 %collective-permute-start.41 = (bf16[704,256]{1,0:T(8,128)(2,1)S(1)}, bf16[704,256]{1,0:T(8,128)(2,1)S(1)}, u32[]{:S(2)}, u32[]{:S(2)}) collective-permute-start(bf16[704,256]{1,0:T(8,128)(2,1)S(1)} %collective-permute-done.34.refs_3_), channel_id=1, source_target_pairs={{0,4},{4,0},{1,5},{5,1},{2,6},{6,2},{3,7},{7,3},{8,12},{12,8},{9,1... | collective-permute-start | bytes 1081352 | tf_op jit(solution)/shard_map/ppermute | solution.py:116
  218.0 3.5 %collective-permute-start.42 = (bf16[1536,512]{1,0:T(8,128)(2,1)S(1)}, bf16[1536,512]{1,0:T(8,128)(2,1)S(1)}, u32[]{:S(2)}, u32[]{:S(2)}) collective-permute-start(bf16[1536,512]{1,0:T(8,128)(2,1)S(1)} %shard_map.125), channel_id=1, source_target_pairs={{0,1},{1,0},{2,3},{3,2},{4,5},{5,4},{6,7},{7,6},{8,9},{9,8},{10,11... | collective-permute-start | bytes 4718600 | tf_op jit(solution)/shard_map/ppermute | solution.py:116
  220.3 4.0 %collective-permute-start.35 = (bf16[1536,512]{1,0:T(8,128)(2,1)S(1)}, bf16[1536,512]{1,0:T(8,128)(2,1)S(1)}, u32[]{:S(2)}, u32[]{:S(2)}) collective-permute-start(bf16[1536,512]{1,0:T(8,128)(2,1)S(1)} %shard_map.123), channel_id=1, source_target_pairs={{0,1},{1,0},{2,3},{3,2},{4,5},{5,4},{6,7},{7,6},{8,9},{9,8},{10,11... | collective-permute-start | bytes 4718600 | tf_op jit(solution)/shard_map/ppermute | solution.py:116
  223.8 19.6 %collective-permute-start.43 = (bf16[1536,256]{1,0:T(8,128)(2,1)S(1)}, bf16[1536,256]{1,0:T(8,128)(2,1)S(1)}, u32[]{:S(2)}, u32[]{:S(2)}) collective-permute-start(bf16[1536,256]{1,0:T(8,128)(2,1)S(1)} %slice.47), channel_id=1, source_target_pairs={{0,2},{2,0},{1,3},{3,1},{4,6},{6,4},{5,7},{7,5},{8,10},{10,8},{9,1... | collective-permute-start | bytes 2359304 | tf_op jit(solution)/shard_map/ppermute | solution.py:116
  226.6 19.4 %collective-permute-start.36 = (bf16[768,512]{1,0:T(8,128)(2,1)S(1)}, bf16[768,512]{1,0:T(8,128)(2,1)S(1)}, u32[]{:S(2)}, u32[]{:S(2)}) collective-permute-start(bf16[768,512]{1,0:T(8,128)(2,1)S(1)} %slice.43), channel_id=1, source_target_pairs={{0,8},{8,0},{1,9},{9,1},{2,10},{10,2},{3,11},{11,3},{4,12},{12,4},... | collective-permute-start | bytes 2359304 | tf_op jit(solution)/shard_map/ppermute | solution.py:116
  244.5 10.3 %collective-permute-start.44 = (bf16[768,256]{1,0:T(8,128)(2,1)S(1)}, bf16[768,256]{1,0:T(8,128)(2,1)S(1)}, u32[]{:S(2)}, u32[]{:S(2)}) collective-permute-start(bf16[768,256]{1,0:T(8,128)(2,1)S(1)} %get-tuple-element.19), channel_id=1, source_target_pairs={{0,8},{8,0},{1,9},{9,1},{2,10},{10,2},{3,11},{11,3},{4,12},{12,4},... | collective-permute-start | bytes 1179656 | tf_op jit(solution)/shard_map/ppermute | solution.py:116
  247.1 10.1 %collective-permute-start.37 = (bf16[768,256]{1,0:T(8,128)(2,1)S(1)}, bf16[768,256]{1,0:T(8,128)(2,1)S(1)}, u32[]{:S(2)}, u32[]{:S(2)}) collective-permute-start(bf16[768,256]{1,0:T(8,128)(2,1)S(1)} %get-tuple-element.21), channel_id=1, source_target_pairs={{0,2},{2,0},{1,3},{3,1},{4,6},{6,4},{5,7},{7,5},{8,10},{10,8},{9,1... | collective-permute-start | bytes 1179656 | tf_op jit(solution)/shard_map/ppermute | solution.py:116
  (23 other events, 354.3 us)

commit v2 on v1

--- a/solution.py
+++ b/solution.py
@@ -13,7 +13,7 @@
 EPS = 1e-06
 LANES = 128
 MIB = 2**20
-PROJECT_MIB, PARTIAL_MIB, HIDDEN_MIB, NEAR_MIB, DOWN_MIB = 60, 60, 56, 56, 24
+PROJECT_MIB, PARTIAL_MIB, HIDDEN_MIB, NEAR_MIB, DOWN_MIB = 60, 60, 60, 50, 24
 
 
 def from_behind(block, axes, count):
@@ -541,7 +541,13 @@
         return own, far, swap(own, "c"), swap(far, "c")
 
     gains = over_tp(norm_gain[None])
-    outs = over_tp(out_weight)
+    rest = out_weight.shape[0] // 2
+    mine = swap(lax.dynamic_slice_in_dim(out_weight, y * rest, rest), "x")
+    theirs = swap(mine, "y")
+    out_x = jnp.concatenate(
+        [jnp.where(y == 0, mine, theirs), jnp.where(y == 0, theirs, mine)], axis=0
+    )
+    outs = out_weight, out_x, swap(out_weight, "c"), swap(out_x, "c")
     normed, middle = project(
         place, over_tp(attended), outs, over_tp(residual), gains,
         rows // 2,
@@ -569,7 +575,7 @@
         rows // 2,
     )
     pieces += last
-    far = far_hidden(where, att2s, outs, res2s, gains, pieces, main, tail, rows // 2)
+    far = far_hidden(where, att2s, outs, res2s, gains, pieces, main, tail, rows)
 
     flags = jnp.stack([c == zl, x == zh]).astype(jnp.int32)
     wide = lambda v: v.astype(jnp.float32)

time: 261 us -> 258 us (0.989)
  starting transfers between devices: 48.1 us -> 37.5 us
  waiting for transfers between devices: 135 us -> 145 us
  local copies, waits for them, and re-layouts: 9.78 us -> 6.68 us
    ppermute x44 -> x45, waiting for transfers between devices: 135 us -> 145 us  [swap(): return lax.ppermute(block, axis, [(0, 1), (1, 0)])]
    ppermute x44 -> x45, starting transfers between devices: 44.7 us -> 34.1 us  [swap(): return lax.ppermute(block, axis, [(0, 1), (1, 0)])]
    unnamed x52 -> x40, local copies, waits for them, and re-layouts: 5.27 us -> 2.08 us
  transfers between devices with their start and end apart: 45 -> 46, of which waited for: 18 -> 20; matrix products, arithmetic and copies ran while one was open for 2% -> 3% of each run, Pallas kernels for 24% -> 23%
where the time goes in v2:
time: 258 us; the launch traced here: 257 us
  waiting for transfers between devices  145 us (56%)
  Pallas kernels  65.1 us (25%)
  starting transfers between devices  37.5 us (15%)
  local copies, waits for them, and re-layouts  6.68 us (3%)
    ppermute x45, waiting for transfers between devices, swap(): return lax.ppermute(block, axis, [(0, 1), (1, 0)])  145 us
    ppermute x45, starting transfers between devices, swap(): return lax.ppermute(block, axis, [(0, 1), (1, 0)])  34.1 us
    pallas_call x1, Pallas kernels, far_hidden(): pl.pallas_call(functools.partial(far_kernel, main, tail, len(pieces)), gr...  16.9 us
    pallas_call x2, Pallas kernels, near_step(): pl.pallas_call(kernel, grid_spec=pltpu.PrefetchScalarGridSpec(num_scalar_...  14.1 us
    pallas_call x1, Pallas kernels, project(): pl.pallas_call(project_kernel, grid_spec=pltpu.PrefetchScalarGridSpec(num...  9.99 us
    pallas_call x4, Pallas kernels, down(): pl.pallas_call(functools.partial(down_kernel, bool(got)), grid_spec=pltpu...  8.82 us
    pallas_call x1, Pallas kernels, attend(): pl.pallas_call(attend_kernel, grid_spec=pltpu.PrefetchScalarGridSpec(num_...  8.16 us
  transfers between devices with their start and end apart: 46, of which 20 were waited for; matrix products, arithmetic and copies ran while one was open for 3% of the time, Pallas kernels for 23%

profile of v2, /device:TPU:0, one launch (start us, length us, event | category | flops | bytes accessed | tf_op | source)
XLA Modules:
  0.0 257.4 jit_solution(11213607645069176770)
XLA Ops:
  0.0 3.0 %collective-permute-start.11 = (f32[1,512]{1,0:T(1,128)}, f32[1,512]{1,0:T(1,128)S(1)}, u32[]{:S(2)}, u32[]{:S(2)}) collective-permute-start(f32[1,512]{1,0:T(1,128)} %bitcast.27), channel_id=1, source_target_pairs={{0,2},{2,0},{1,3},{3,1},{4,6},{6,4},{5,7},{7,5},{8,10},{10,8},{9,1... | collective-permute-start | bytes 6152 | tf_op jit(solution)/shard_map/ppermute | solution.py:116
  3.0 2.6 shard_map.119
  5.5 1.6 collective-permute-start.15
  8.6 3.4 %collective-permute-start = (bf16[128,128]{1,0:T(8,128)(2,1)S(1)}, bf16[128,128]{1,0:T(8,128)(2,1)S(1)}, u32[]{:S(2)}, u32[]{:S(2)}) collective-permute-start(bf16[128,128]{1,0:T(8,128)(2,1)S(1)} %pad_maximum_fusion.1), channel_id=1, source_target_pairs={{0,4},{4,8},{8,12},{12,16},{16,20},{20,24},{24,28},{1,5},{5,9},{9,... | collective-permute-start | bytes 98312 | tf_op jit(solution)/shard_map/ppermute | solution.py:20
  12.5 2.0 shard_map.122
  14.6 1.6 collective-permute-start.33
  16.2 2.6 %collective-permute-start.34 = (bf16[704,256]{1,0:T(8,128)(2,1)}, bf16[704,256]{1,0:T(8,128)(2,1)S(1)}, u32[]{:S(2)}, u32[]{:S(2)}) collective-permute-start(bf16[704,256]{1,0:T(8,128)(2,1)} %get-tuple-element.17.refs_0_), channel_id=1, source_target_pairs={{0,16},{16,0},{1,17},{17,1},{2,18},{18,2},{3,19},{19,3},{4,20},{20... | collective-permute-start | bytes 1081352 | tf_op jit(solution)/shard_map/ppermute | solution.py:116
  20.5 8.2 %attend.1.refs_0_ = bf16[768,256]{1,0:T(8,128)(2,1)} custom-call(s32[1]{0:T(128)} %bitcast.5.place_ref, f32[4]{0:T(128)} %sink_ref.1, bf16[768,256]{1,0:T(8,128)(2,1)} %q_ref.1, bf16[64,768]{1,0:T(8,128)(2,1)} %bitcast.23, bf16[64,768]{1,0:T(8,128)(2,1)} %bitcast.25, bf16[128,128]{1,0:T(8,128)(2,1)} %copy-done.16, f32[1,64]{1,0:T(1,128)} %bitcast.31, ...), custom_call_target="tpu_custom_call" | custom-call | flops 2516582400 | bytes 786432 | tf_op jit(solution)/shard_map/attend/pallas_call | solution.py:179
  28.7 10.2 %collective-permute-done.16.refs_3_.refs_19_ = bf16[128,1408]{1,0:T(8,128)(2,1)} collective-permute-done((bf16[128,1408]{1,0:T(8,128)(2,1)}, bf16[128,1408]{1,0:T(8,128)(2,1)}, u32[]{:S(2)}, u32[]{:S(2)}) %collective-permute-start.16) | collective-permute-done | bytes 360480 | tf_op jit(solution)/shard_map/ppermute | solution.py:116
  38.8 7.6 %collective-permute-done.33.refs_1_ = bf16[704,256]{1,0:T(8,128)(2,1)S(1)} collective-permute-done((bf16[704,256]{1,0:T(8,128)(2,1)}, bf16[704,256]{1,0:T(8,128)(2,1)S(1)}, u32[]{:S(2)}, u32[]{:S(2)}) %collective-permute-start.33) | collective-permute-done | bytes 360480 | tf_op jit(solution)/shard_map/ppermute | solution.py:116
  46.6 2.1 collective-permute-start.5
  48.7 14.2 %collective-permute-done.25.refs_0_ = bf16[768,256]{1,0:T(8,128)(2,1)} collective-permute-done((bf16[768,256]{1,0:T(8,128)(2,1)}, bf16[768,256]{1,0:T(8,128)(2,1)}, u32[]{:S(2)}, u32[]{:S(2)}) %collective-permute-start.25) | collective-permute-done | bytes 393248 | tf_op jit(solution)/shard_map/ppermute | solution.py:116
  62.9 3.5 %collective-permute-start.21 = (bf16[128,1408]{1,0:T(8,128)(2,1)}, bf16[128,1408]{1,0:T(8,128)(2,1)S(1)}, u32[]{:S(2)}, u32[]{:S(2)}) collective-permute-start(bf16[128,1408]{1,0:T(8,128)(2,1)} %copy-done.14), channel_id=1, source_target_pairs={{0,16},{16,0},{1,17},{17,1},{2,18},{18,2},{3,19},{19,3},{4,20},{20... | collective-permute-start | bytes 1081352 | tf_op jit(solution)/shard_map/ppermute | solution.py:116
  66.4 1.6 collective-permute-start.17
  68.5 22.8 %collective-permute-done.21.refs_0_.refs_24_ = bf16[128,1408]{1,0:T(8,128)(2,1)S(1)} collective-permute-done((bf16[128,1408]{1,0:T(8,128)(2,1)}, bf16[128,1408]{1,0:T(8,128)(2,1)S(1)}, u32[]{:S(2)}, u32[]{:S(2)}) %collective-permute-start.21) | collective-permute-done | bytes 360480 | tf_op jit(solution)/shard_map/ppermute | solution.py:116
  91.3 6.8 %collective-permute-done.22.refs_1_.refs_25_ = bf16[128,1408]{1,0:T(8,128)(2,1)S(1)} collective-permute-done((bf16[128,1408]{1,0:T(8,128)(2,1)}, bf16[128,1408]{1,0:T(8,128)(2,1)S(1)}, u32[]{:S(2)}, u32[]{:S(2)}) %collective-permute-start.22) | collective-permute-done | bytes 360480 | tf_op jit(solution)/shard_map/ppermute | solution.py:116
  98.6 1.6 collective-permute-start.18
  100.3 9.5 %collective-permute-done.18.refs_5_.refs_21_ = bf16[128,1408]{1,0:T(8,128)(2,1)} collective-permute-done((bf16[128,1408]{1,0:T(8,128)(2,1)}, bf16[128,1408]{1,0:T(8,128)(2,1)}, u32[]{:S(2)}, u32[]{:S(2)}) %collective-permute-start.18) | collective-permute-done | bytes 360480 | tf_op jit(solution)/shard_map/ppermute | solution.py:116
  109.8 1.5 collective-permute-start.26
  111.3 1.2 pad_maximum_fusion.refs_5_
  112.4 2.5 collective-permute-done.29.refs_8_
  115.0 3.9 %collective-permute-done.8.refs_9_ = bf16[768,512]{1,0:T(8,128)(2,1)} collective-permute-done((bf16[768,512]{1,0:T(8,128)(2,1)}, bf16[768,512]{1,0:T(8,128)(2,1)}, u32[]{:S(2)}, u32[]{:S(2)}) %collective-permute-start.8) | collective-permute-done | bytes 786464 | tf_op jit(solution)/shard_map/ppermute | solution.py:116
  119.3 7.9 %collective-permute-done.26.refs_1_ = bf16[768,256]{1,0:T(8,128)(2,1)} collective-permute-done((bf16[768,256]{1,0:T(8,128)(2,1)}, bf16[768,256]{1,0:T(8,128)(2,1)}, u32[]{:S(2)}, u32[]{:S(2)}) %collective-permute-start.26) | collective-permute-done | bytes 393248 | tf_op jit(solution)/shard_map/ppermute | solution.py:116
  127.2 2.1 collective-permute-done.3.refs_3_
  129.3 1.5 collective-permute-start.20
  131.4 10.7 %collective-permute-done.30.refs_9_ = bf16[768,512]{1,0:T(8,128)(2,1)} collective-permute-done((bf16[768,512]{1,0:T(8,128)(2,1)}, bf16[768,512]{1,0:T(8,128)(2,1)}, u32[]{:S(2)}, u32[]{:S(2)}) %collective-permute-start.30) | collective-permute-done | bytes 786464 | tf_op jit(solution)/shard_map/ppermute | solution.py:116
  142.1 1.4 collective-permute-start.24
  145.3 10.0 %shard_map.118 = (bf16[768,2048]{1,0:T(8,128)(2,1)}, bf16[768,512]{1,0:T(8,128)(2,1)}) custom-call(s32[4]{0:T(128)} %pad_add_fusion.place_ref, bf16[768,256]{1,0:T(8,128)(2,1)} %attend.1.refs_0_, bf16[768,256]{1,0:T(8,128)(2,1)} %copy-done.12, bf16[768,256]{1,0:T(8,128)(2,1)} %copy-done.13, bf16[768,256]{1,0:T(8,128)(2,1)} %collective-permute-done.3.refs_3_, ...), custom_call_target="tpu_custom_call" | custom-call | flops 3221225472 | bytes 6291456 | tf_op jit(solution)/shard_map/pallas_call | solution.py:283
  155.3 0.9 collective-permute-done.23.refs_2_.refs_26_
  156.2 6.9 %collective-permute-done.24.refs_3_.refs_27_ = bf16[128,1408]{1,0:T(8,128)(2,1)S(1)} collective-permute-done((bf16[128,1408]{1,0:T(8,128)(2,1)S(1)}, bf16[128,1408]{1,0:T(8,128)(2,1)S(1)}, u32[]{:S(2)}, u32[]{:S(2)}) %collective-permute-start.24) | collective-permute-done | bytes 360480 | tf_op jit(solution)/shard_map/ppermute | solution.py:116
  163.7 9.2 %shard_map.120.acts_ref = f32[768,1408]{1,0:T(8,128)} custom-call(s32[12]{0:T(128)} %concatenate.12.place_ref, bf16[768,2048]{1,0:T(8,128)(2,1)} %get-tuple-element.13.x_ref, bf16[256,1408]{1,0:T(8,128)(2,1)} %get-tuple-element.14.refs_0_.refs_16_, bf16[256,1408]{1,0:T(8,128)(2,1)} %collective-permute-done.14.refs_1_.refs_17_, bf16[128,1408]{1,0:T(8,128)(2,1)} %copy-done.14, ...), custom_call_target="tpu_custom_call" | custom-call | flops 3538944000 | bytes 3072000 | tf_op jit(solution)/shard_map/pallas_call | solution.py:391
  172.9 4.8 %shard_map.121.near_ref = bf16[768,704]{1,0:T(8,128)(2,1)S(1)} custom-call(s32[12]{0:T(128)S(1)} %copy-done.6, bf16[768,2048]{1,0:T(8,128)(2,1)} %get-tuple-element.13.x_ref, f32[768,1408]{1,0:T(8,128)} %shard_map.120.acts_ref, bf16[128,1408]{1,0:T(8,128)(2,1)S(1)} %collective-permute-done.21.refs_0_.refs_24_, ...), custom_call_target="tpu_custom_call" | custom-call | flops 1179648000 | bytes 3072000 | tf_op jit(solution)/shard_map/pallas_call | solution.py:391
  177.8 1.6 collective-permute-start.39
  179.9 1.5 collective-permute-start.41
  181.9 16.9 %far_hidden.1.far_ref = bf16[768,704]{1,0:T(8,128)(2,1)} custom-call(s32[12]{0:T(128)} %concatenate.12.place_ref, bf16[768,256]{1,0:T(8,128)(2,1)} %collective-permute-done.25.refs_0_, bf16[768,256]{1,0:T(8,128)(2,1)} %collective-permute-done.26.refs_1_, bf16[768,256]{1,0:T(8,128)(2,1)} %collective-permute-done.27.refs_2_, ...), custom_call_target="tpu_custom_call" | custom-call | flops 8858370048 | bytes 8650752 | tf_op jit(solution)/shard_map/far_hidden/pallas_call | solution.py:347
  198.8 5.8 %collective-permute-done.41.refs_2_ = bf16[704,256]{1,0:T(8,128)(2,1)S(1)} collective-permute-done((bf16[704,256]{1,0:T(8,128)(2,1)S(1)}, bf16[704,256]{1,0:T(8,128)(2,1)S(1)}, u32[]{:S(2)}, u32[]{:S(2)}) %collective-permute-start.41) | collective-permute-done | bytes 360480 | tf_op jit(solution)/shard_map/ppermute | solution.py:116
  204.6 6.8 %collective-permute-done.42.refs_3_ = bf16[704,256]{1,0:T(8,128)(2,1)S(1)} collective-permute-done((bf16[704,256]{1,0:T(8,128)(2,1)S(1)}, bf16[704,256]{1,0:T(8,128)(2,1)S(1)}, u32[]{:S(2)}, u32[]{:S(2)}) %collective-permute-start.42) | collective-permute-done | bytes 360480 | tf_op jit(solution)/shard_map/ppermute | solution.py:116
  211.4 1.3 copy-done
  212.7 2.2 shard_map.125
  215.0 2.2 shard_map.123
  218.4 2.2 shard_map.126
  221.2 2.2 shard_map.124
  223.6 16.7 %collective-permute-done.44 = bf16[1536,256]{1,0:T(8,128)(2,1)S(1)} collective-permute-done((bf16[1536,256]{1,0:T(8,128)(2,1)S(1)}, bf16[1536,256]{1,0:T(8,128)(2,1)S(1)}, u32[]{:S(2)}, u32[]{:S(2)}) %collective-permute-start.44) | collective-permute-done | bytes 786464 | tf_op jit(solution)/shard_map/ppermute | solution.py:116
  241.3 1.6 collective-permute-done.37
  244.0 2.1 collective-permute-start.38
  246.1 5.5 %collective-permute-done.45.behind_got = bf16[768,256]{1,0:T(8,128)(2,1)S(1)} collective-permute-done((bf16[768,256]{1,0:T(8,128)(2,1)S(1)}, bf16[768,256]{1,0:T(8,128)(2,1)S(1)}, u32[]{:S(2)}, u32[]{:S(2)}) %collective-permute-start.45) | collective-permute-done | bytes 393248 | tf_op jit(solution)/shard_map/ppermute | solution.py:116
  251.6 2.5 collective-permute-done.38.ahead_got
  254.8 2.6 %finish.1 = bf16[768,512]{1,0:T(8,128)(2,1)} custom-call(s32[1]{0:T(128)} %bitcast.flag_ref, bf16[768,512]{1,0:T(8,128)(2,1)} %get-tuple-element.12.middle_ref, bf16[768,256]{1,0:T(8,128)(2,1)} %get-tuple-element.24.ahead_ref, bf16[768,256]{1,0:T(8,128)(2,1)} %copy-done.8, bf16[768,256]{1,0:T(8,128)(2,1)} %get-tuple-element.22.behind_ref, ...), custom_call_target="tpu_custom_call" | custom-call | flops 3145728 | bytes 3145728 | tf_op jit(solution)/shard_map/finish/pallas_call | solution.py:476
  (112 shorter events, 14.3 us)
Async XLA Ops:
  0.0 12.5 %collective-permute-start.11 = (f32[1,512]{1,0:T(1,128)}, f32[1,512]{1,0:T(1,128)S(1)}, u32[]{:S(2)}, u32[]{:S(2)}) collective-permute-start(f32[1,512]{1,0:T(1,128)} %bitcast.27), channel_id=1, source_target_pairs={{0,2},{2,0},{1,3},{3,1},{4,6},{6,4},{5,7},{7,5},{8,10},{10,8},{9,1... | collective-permute-start | bytes 6152 | tf_op jit(solution)/shard_map/ppermute | solution.py:116
  3.0 11.6 %collective-permute-start.12 = (f32[1,512]{1,0:T(1,128)}, f32[1,512]{1,0:T(1,128)S(1)}, u32[]{:S(2)}, u32[]{:S(2)}) collective-permute-start(f32[1,512]{1,0:T(1,128)} %bitcast.28), channel_id=1, source_target_pairs={{0,1},{1,0},{2,3},{3,2},{4,5},{5,4},{6,7},{7,6},{8,9},{9,8},{10,11... | collective-permute-start | bytes 6152 | tf_op jit(solution)/shard_map/ppermute | solution.py:116
  5.5 14.6 %collective-permute-start.15 = (bf16[128,1408]{1,0:T(8,128)(2,1)}, bf16[128,1408]{1,0:T(8,128)(2,1)S(1)}, u32[]{:S(2)}, u32[]{:S(2)}) collective-permute-start(bf16[128,1408]{1,0:T(8,128)(2,1)} %get-tuple-element.15), channel_id=1, source_target_pairs={{0,8},{8,0},{1,9},{9,1},{2,10},{10,2},{3,11},{11,3},{4,12},{12,4},... | collective-permute-start | bytes 1081352 | tf_op jit(solution)/shard_map/ppermute | solution.py:116
  8.6 10.3 %collective-permute-start = (bf16[128,128]{1,0:T(8,128)(2,1)S(1)}, bf16[128,128]{1,0:T(8,128)(2,1)S(1)}, u32[]{:S(2)}, u32[]{:S(2)}) collective-permute-start(bf16[128,128]{1,0:T(8,128)(2,1)S(1)} %pad_maximum_fusion.1), channel_id=1, source_target_pairs={{0,4},{4,8},{8,12},{12,16},{16,20},{20,24},{24,28},{1,5},{5,9},{9,... | collective-permute-start | bytes 98312 | tf_op jit(solution)/shard_map/ppermute | solution.py:20
  12.0 26.8 %collective-permute-start.16 = (bf16[128,1408]{1,0:T(8,128)(2,1)}, bf16[128,1408]{1,0:T(8,128)(2,1)}, u32[]{:S(2)}, u32[]{:S(2)}) collective-permute-start(bf16[128,1408]{1,0:T(8,128)(2,1)} %get-tuple-element.16), channel_id=1, source_target_pairs={{0,8},{8,0},{1,9},{9,1},{2,10},{10,2},{3,11},{11,3},{4,12},{12,4},... | collective-permute-start | bytes 1081352 | tf_op jit(solution)/shard_map/ppermute | solution.py:116
  12.5 3.7 %collective-permute-start.13 = (f32[1,512]{1,0:T(1,128)S(1)}, f32[1,512]{1,0:T(1,128)S(1)}, u32[]{:S(2)}, u32[]{:S(2)}) collective-permute-start(f32[1,512]{1,0:T(1,128)S(1)} %collective-permute-done.11.refs_13_), channel_id=1, source_target_pairs={{0,1},{1,0},{2,3},{3,2},{4,5},{5,4},{6,7},{7,6},{8,9},{9,8},{10,11... | collective-permute-start | bytes 6152 | tf_op jit(solution)/shard_map/ppermute | solution.py:116
  14.6 31.9 %collective-permute-start.33 = (bf16[704,256]{1,0:T(8,128)(2,1)}, bf16[704,256]{1,0:T(8,128)(2,1)S(1)}, u32[]{:S(2)}, u32[]{:S(2)}) collective-permute-start(bf16[704,256]{1,0:T(8,128)(2,1)} %get-tuple-element.18), channel_id=1, source_target_pairs={{0,8},{8,0},{1,9},{9,1},{2,10},{10,2},{3,11},{11,3},{4,12},{12,4},... | collective-permute-start | bytes 1081352 | tf_op jit(solution)/shard_map/ppermute | solution.py:116
  16.2 30.3 %collective-permute-start.34 = (bf16[704,256]{1,0:T(8,128)(2,1)}, bf16[704,256]{1,0:T(8,128)(2,1)S(1)}, u32[]{:S(2)}, u32[]{:S(2)}) collective-permute-start(bf16[704,256]{1,0:T(8,128)(2,1)} %get-tuple-element.17.refs_0_), channel_id=1, source_target_pairs={{0,16},{16,0},{1,17},{17,1},{2,18},{18,2},{3,19},{19,3},{4,20},{20... | collective-permute-start | bytes 1081352 | tf_op jit(solution)/shard_map/ppermute | solution.py:116
  18.9 27.7 %collective-permute-start.4 = (bf16[128,2048]{1,0:T(8,128)(2,1)S(1)}, bf16[128,2048]{1,0:T(8,128)(2,1)S(1)}, u32[]{:S(2)}, u32[]{:S(2)}) collective-permute-start(bf16[128,2048]{1,0:T(8,128)(2,1)S(1)} %constant_dynamic-slice_fusion), channel_id=1, source_target_pairs={{0,2},{2,0},{1,3},{3,1},{4,6},{6,4},{5,7},{7,5},{8,10},{10,8},{9,1... | collective-permute-start | bytes 1572872 | tf_op jit(solution)/shard_map/ppermute | solution.py:116
  20.2 47.9 %collective-permute-start.19 = (bf16[256,1408]{1,0:T(8,128)(2,1)}, bf16[256,1408]{1,0:T(8,128)(2,1)}, u32[]{:S(2)}, u32[]{:S(2)}) collective-permute-start(bf16[256,1408]{1,0:T(8,128)(2,1)} %get-tuple-element.14.refs_0_.refs_16_), channel_id=1, source_target_pairs={{0,16},{16,0},{1,17},{17,1},{2,18},{18,2},{3,19},{19,3},{4,20},{20... | collective-permute-start | bytes 2162696 | tf_op jit(solution)/shard_map/ppermute | solution.py:116
  38.8 24.0 %collective-permute-start.25 = (bf16[768,256]{1,0:T(8,128)(2,1)}, bf16[768,256]{1,0:T(8,128)(2,1)}, u32[]{:S(2)}, u32[]{:S(2)}) collective-permute-start(bf16[768,256]{1,0:T(8,128)(2,1)} %attend.1.refs_0_), channel_id=1, source_target_pairs={{0,8},{8,0},{1,9},{9,1},{2,10},{10,2},{3,11},{11,3},{4,12},{12,4},... | collective-permute-start | bytes 1179656 | tf_op jit(solution)/shard_map/ppermute | solution.py:116
  46.5 19.9 %collective-permute-start.1 = (bf16[768,256]{1,0:T(8,128)(2,1)}, bf16[768,256]{1,0:T(8,128)(2,1)S(1)}, u32[]{:S(2)}, u32[]{:S(2)}) collective-permute-start(bf16[768,256]{1,0:T(8,128)(2,1)} %attend.1.refs_0_), channel_id=1, source_target_pairs={{0,2},{2,0},{1,3},{3,1},{4,6},{6,4},{5,7},{7,5},{8,10},{10,8},{9,1... | collective-permute-start | bytes 1179656 | tf_op jit(solution)/shard_map/ppermute | solution.py:116
  46.5 19.9 %collective-permute-start.2 = (bf16[768,256]{1,0:T(8,128)(2,1)}, bf16[768,256]{1,0:T(8,128)(2,1)S(1)}, u32[]{:S(2)}, u32[]{:S(2)}) collective-permute-start(bf16[768,256]{1,0:T(8,128)(2,1)} %attend.1.refs_0_), channel_id=1, source_target_pairs={{0,1},{1,0},{2,3},{3,2},{4,5},{5,4},{6,7},{7,6},{8,9},{9,8},{10,11... | collective-permute-start | bytes 1179656 | tf_op jit(solution)/shard_map/ppermute | solution.py:116
  46.6 52.1 %collective-permute-start.5 = (bf16[128,2048]{1,0:T(8,128)(2,1)S(1)}, bf16[128,2048]{1,0:T(8,128)(2,1)S(1)}, u32[]{:S(2)}, u32[]{:S(2)}) collective-permute-start(bf16[128,2048]{1,0:T(8,128)(2,1)S(1)} %collective-permute-done.4), channel_id=1, source_target_pairs={{0,4},{4,0},{1,5},{5,1},{2,6},{6,2},{3,7},{7,3},{8,12},{12,8},{9,1... | collective-permute-start | bytes 1572872 | tf_op jit(solution)/shard_map/ppermute | solution.py:116
  62.9 28.4 %collective-permute-start.21 = (bf16[128,1408]{1,0:T(8,128)(2,1)}, bf16[128,1408]{1,0:T(8,128)(2,1)S(1)}, u32[]{:S(2)}, u32[]{:S(2)}) collective-permute-start(bf16[128,1408]{1,0:T(8,128)(2,1)} %copy-done.14), channel_id=1, source_target_pairs={{0,16},{16,0},{1,17},{17,1},{2,18},{18,2},{3,19},{19,3},{4,20},{20... | collective-permute-start | bytes 1081352 | tf_op jit(solution)/shard_map/ppermute | solution.py:116
  66.4 31.7 %collective-permute-start.22 = (bf16[128,1408]{1,0:T(8,128)(2,1)}, bf16[128,1408]{1,0:T(8,128)(2,1)S(1)}, u32[]{:S(2)}, u32[]{:S(2)}) collective-permute-start(bf16[128,1408]{1,0:T(8,128)(2,1)} %collective-permute-done.16.refs_3_.refs_19_), channel_id=1, source_target_pairs={{0,16},{16,0},{1,17},{17,1},{2,18},{18,2},{3,19},{19,3},{4,20},{20... | collective-permute-start | bytes 1081352 | tf_op jit(solution)/shard_map/ppermute | solution.py:116
  66.4 32.2 %collective-permute-start.17 = (bf16[128,1408]{1,0:T(8,128)(2,1)}, bf16[128,1408]{1,0:T(8,128)(2,1)S(1)}, u32[]{:S(2)}, u32[]{:S(2)}) collective-permute-start(bf16[128,1408]{1,0:T(8,128)(2,1)} %copy-done.14), channel_id=1, source_target_pairs={{0,4},{4,0},{1,5},{5,1},{2,6},{6,2},{3,7},{7,3},{8,12},{12,8},{9,1... | collective-permute-start | bytes 1081352 | tf_op jit(solution)/shard_map/ppermute | solution.py:116
  68.0 41.7 %collective-permute-start.14 = (bf16[256,1408]{1,0:T(8,128)(2,1)}, bf16[256,1408]{1,0:T(8,128)(2,1)}, u32[]{:S(2)}, u32[]{:S(2)}) collective-permute-start(bf16[256,1408]{1,0:T(8,128)(2,1)} %get-tuple-element.14.refs_0_.refs_16_), channel_id=1, source_target_pairs={{0,4},{4,0},{1,5},{5,1},{2,6},{6,2},{3,7},{7,3},{8,12},{12,8},{9,1... | collective-permute-start | bytes 2162696 | tf_op jit(solution)/shard_map/ppermute | solution.py:116
  91.3 81.6 %copy-start.2 = (bf16[128,1408]{1,0:T(8,128)(2,1)}, bf16[128,1408]{1,0:T(8,128)(2,1)S(1)}, u32[]{:S(2)}) copy-start(bf16[128,1408]{1,0:T(8,128)(2,1)S(1)} %collective-permute-done.21.refs_0_.refs_24_) | copy-start | bytes 1081348
  91.3 23.6 %collective-permute-start.29 = (bf16[768,512]{1,0:T(8,128)(2,1)}, bf16[768,512]{1,0:T(8,128)(2,1)}, u32[]{:S(2)}, u32[]{:S(2)}) collective-permute-start(bf16[768,512]{1,0:T(8,128)(2,1)} %refs_8_.1), channel_id=1, source_target_pairs={{0,8},{8,0},{1,9},{9,1},{2,10},{10,2},{3,11},{11,3},{4,12},{12,4},... | collective-permute-start | bytes 2359304 | tf_op jit(solution)/shard_map/ppermute | solution.py:116
  98.1 74.8 %copy-start.3 = (bf16[128,1408]{1,0:T(8,128)(2,1)}, bf16[128,1408]{1,0:T(8,128)(2,1)S(1)}, u32[]{:S(2)}) copy-start(bf16[128,1408]{1,0:T(8,128)(2,1)S(1)} %collective-permute-done.22.refs_1_.refs_25_) | copy-start | bytes 1081348
  98.1 20.7 %collective-permute-start.8 = (bf16[768,512]{1,0:T(8,128)(2,1)}, bf16[768,512]{1,0:T(8,128)(2,1)}, u32[]{:S(2)}, u32[]{:S(2)}) collective-permute-start(bf16[768,512]{1,0:T(8,128)(2,1)} %refs_8_.1), channel_id=1, source_target_pairs={{0,2},{2,0},{1,3},{3,1},{4,6},{6,4},{5,7},{7,5},{8,10},{10,8},{9,1... | collective-permute-start | bytes 2359304 | tf_op jit(solution)/shard_map/ppermute | solution.py:116
  98.6 20.7 %collective-permute-start.9 = (bf16[768,512]{1,0:T(8,128)(2,1)}, bf16[768,512]{1,0:T(8,128)(2,1)}, u32[]{:S(2)}, u32[]{:S(2)}) collective-permute-start(bf16[768,512]{1,0:T(8,128)(2,1)} %refs_8_.1), channel_id=1, source_target_pairs={{0,1},{1,0},{2,3},{3,2},{4,5},{5,4},{6,7},{7,6},{8,9},{9,8},{10,11... | collective-permute-start | bytes 2359304 | tf_op jit(solution)/shard_map/ppermute | solution.py:116
  98.6 11.1 %collective-permute-start.18 = (bf16[128,1408]{1,0:T(8,128)(2,1)}, bf16[128,1408]{1,0:T(8,128)(2,1)}, u32[]{:S(2)}, u32[]{:S(2)}) collective-permute-start(bf16[128,1408]{1,0:T(8,128)(2,1)} %collective-permute-done.16.refs_3_.refs_19_), channel_id=1, source_target_pairs={{0,4},{4,0},{1,5},{5,1},{2,6},{6,2},{3,7},{7,3},{8,12},{12,8},{9,1... | collective-permute-start | bytes 1081352 | tf_op jit(solution)/shard_map/ppermute | solution.py:116
  109.8 21.1 %collective-permute-start.6 = (bf16[256,2048]{1,0:T(8,128)(2,1)}, bf16[256,2048]{1,0:T(8,128)(2,1)}, u32[]{:S(2)}, u32[]{:S(2)}) collective-permute-start(bf16[256,2048]{1,0:T(8,128)(2,1)} %refs_4_.3), channel_id=1, source_target_pairs={{0,1},{1,0},{2,3},{3,2},{4,5},{5,4},{6,7},{7,6},{8,9},{9,8},{10,11... | collective-permute-start | bytes 3145736 | tf_op jit(solution)/shard_map/ppermute | solution.py:116
  109.8 17.5 %collective-permute-start.26 = (bf16[768,256]{1,0:T(8,128)(2,1)}, bf16[768,256]{1,0:T(8,128)(2,1)}, u32[]{:S(2)}, u32[]{:S(2)}) collective-permute-start(bf16[768,256]{1,0:T(8,128)(2,1)} %collective-permute-done.25.refs_0_), channel_id=1, source_target_pairs={{0,2},{2,0},{1,3},{3,1},{4,6},{6,4},{5,7},{7,5},{8,10},{10,8},{9,1... | collective-permute-start | bytes 1179656 | tf_op jit(solution)/shard_map/ppermute | solution.py:116
  114.9 28.6 %collective-permute-start.7 = (bf16[256,2048]{1,0:T(8,128)(2,1)}, bf16[256,2048]{1,0:T(8,128)(2,1)}, u32[]{:S(2)}, u32[]{:S(2)}) collective-permute-start(bf16[256,2048]{1,0:T(8,128)(2,1)} %pad_maximum_fusion.refs_5_), channel_id=1, source_target_pairs={{0,1},{1,0},{2,3},{3,2},{4,5},{5,4},{6,7},{7,6},{8,9},{9,8},{10,11... | collective-permute-start | bytes 3145736 | tf_op jit(solution)/shard_map/ppermute | solution.py:116
  118.8 23.3 %collective-permute-start.30 = (bf16[768,512]{1,0:T(8,128)(2,1)}, bf16[768,512]{1,0:T(8,128)(2,1)}, u32[]{:S(2)}, u32[]{:S(2)}) collective-permute-start(bf16[768,512]{1,0:T(8,128)(2,1)} %collective-permute-done.29.refs_8_), channel_id=1, source_target_pairs={{0,2},{2,0},{1,3},{3,1},{4,6},{6,4},{5,7},{7,5},{8,10},{10,8},{9,1... | collective-permute-start | bytes 2359304 | tf_op jit(solution)/shard_map/ppermute | solution.py:116
  119.3 24.2 %collective-permute-start.10 = (bf16[768,512]{1,0:T(8,128)(2,1)}, bf16[768,512]{1,0:T(8,128)(2,1)S(1)}, u32[]{:S(2)}, u32[]{:S(2)}) collective-permute-start(bf16[768,512]{1,0:T(8,128)(2,1)} %collective-permute-done.8.refs_9_), channel_id=1, source_target_pairs={{0,1},{1,0},{2,3},{3,2},{4,5},{5,4},{6,7},{7,6},{8,9},{9,8},{10,11... | collective-permute-start | bytes 2359304 | tf_op jit(solution)/shard_map/ppermute | solution.py:116
  127.2 2.1 collective-permute-start.3
  129.3 33.8 %collective-permute-start.20 = (bf16[256,1408]{1,0:T(8,128)(2,1)}, bf16[256,1408]{1,0:T(8,128)(2,1)}, u32[]{:S(2)}, u32[]{:S(2)}) collective-permute-start(bf16[256,1408]{1,0:T(8,128)(2,1)} %collective-permute-done.19.refs_6_.refs_22_), channel_id=1, source_target_pairs={{0,4},{4,0},{1,5},{5,1},{2,6},{6,2},{3,7},{7,3},{8,12},{12,8},{9,1... | collective-permute-start | bytes 2162696 | tf_op jit(solution)/shard_map/ppermute | solution.py:116
  130.9 25.3 %collective-permute-start.23 = (bf16[128,1408]{1,0:T(8,128)(2,1)S(1)}, bf16[128,1408]{1,0:T(8,128)(2,1)S(1)}, u32[]{:S(2)}, u32[]{:S(2)}) collective-permute-start(bf16[128,1408]{1,0:T(8,128)(2,1)S(1)} %collective-permute-done.21.refs_0_.refs_24_), channel_id=1, source_target_pairs={{0,4},{4,0},{1,5},{5,1},{2,6},{6,2},{3,7},{7,3},{8,12},{12,8},{9,1... | collective-permute-start | bytes 1081352 | tf_op jit(solution)/shard_map/ppermute | solution.py:116
  142.1 21.0 %collective-permute-start.24 = (bf16[128,1408]{1,0:T(8,128)(2,1)S(1)}, bf16[128,1408]{1,0:T(8,128)(2,1)S(1)}, u32[]{:S(2)}, u32[]{:S(2)}) collective-permute-start(bf16[128,1408]{1,0:T(8,128)(2,1)S(1)} %collective-permute-done.22.refs_1_.refs_25_), channel_id=1, source_target_pairs={{0,4},{4,0},{1,5},{5,1},{2,6},{6,2},{3,7},{7,3},{8,12},{12,8},{9,1... | collective-permute-start | bytes 1081352 | tf_op jit(solution)/shard_map/ppermute | solution.py:116
  143.5 37.9 %collective-permute-start.31 = (bf16[768,512]{1,0:T(8,128)(2,1)}, bf16[768,512]{1,0:T(8,128)(2,1)}, u32[]{:S(2)}, u32[]{:S(2)}) collective-permute-start(bf16[768,512]{1,0:T(8,128)(2,1)} %collective-permute-done.29.refs_8_), channel_id=1, source_target_pairs={{0,1},{1,0},{2,3},{3,2},{4,5},{5,4},{6,7},{7,6},{8,9},{9,8},{10,11... | collective-permute-start | bytes 2359304 | tf_op jit(solution)/shard_map/ppermute | solution.py:116
  143.6 38.4 %collective-permute-start.32 = (bf16[768,512]{1,0:T(8,128)(2,1)}, bf16[768,512]{1,0:T(8,128)(2,1)}, u32[]{:S(2)}, u32[]{:S(2)}) collective-permute-start(bf16[768,512]{1,0:T(8,128)(2,1)} %collective-permute-done.30.refs_9_), channel_id=1, source_target_pairs={{0,1},{1,0},{2,3},{3,2},{4,5},{5,4},{6,7},{7,6},{8,9},{9,8},{10,11... | collective-permute-start | bytes 2359304 | tf_op jit(solution)/shard_map/ppermute | solution.py:116
  156.2 21.5 %collective-permute-start.35 = (bf16[704,256]{1,0:T(8,128)(2,1)S(1)}, bf16[704,256]{1,0:T(8,128)(2,1)S(1)}, u32[]{:S(2)}, u32[]{:S(2)}) collective-permute-start(bf16[704,256]{1,0:T(8,128)(2,1)S(1)} %collective-permute-done.33.refs_1_), channel_id=1, source_target_pairs={{0,16},{16,0},{1,17},{17,1},{2,18},{18,2},{3,19},{19,3},{4,20},{20... | collective-permute-start | bytes 1081352 | tf_op jit(solution)/shard_map/ppermute | solution.py:116
  163.1 16.2 %collective-permute-start.27 = (bf16[768,256]{1,0:T(8,128)(2,1)}, bf16[768,256]{1,0:T(8,128)(2,1)}, u32[]{:S(2)}, u32[]{:S(2)}) collective-permute-start(bf16[768,256]{1,0:T(8,128)(2,1)} %collective-permute-done.25.refs_0_), channel_id=1, source_target_pairs={{0,1},{1,0},{2,3},{3,2},{4,5},{5,4},{6,7},{7,6},{8,9},{9,8},{10,11... | collective-permute-start | bytes 1179656 | tf_op jit(solution)/shard_map/ppermute | solution.py:116
  163.1 16.7 %collective-permute-start.28 = (bf16[768,256]{1,0:T(8,128)(2,1)}, bf16[768,256]{1,0:T(8,128)(2,1)}, u32[]{:S(2)}, u32[]{:S(2)}) collective-permute-start(bf16[768,256]{1,0:T(8,128)(2,1)} %collective-permute-done.26.refs_1_), channel_id=1, source_target_pairs={{0,1},{1,0},{2,3},{3,2},{4,5},{5,4},{6,7},{7,6},{8,9},{9,8},{10,11... | collective-permute-start | bytes 1179656 | tf_op jit(solution)/shard_map/ppermute | solution.py:116
  177.8 21.0 %collective-permute-start.39 = (bf16[704,256]{1,0:T(8,128)(2,1)S(1)}, bf16[704,256]{1,0:T(8,128)(2,1)S(1)}, u32[]{:S(2)}, u32[]{:S(2)}) collective-permute-start(bf16[704,256]{1,0:T(8,128)(2,1)S(1)} %copy-done.1), channel_id=1, source_target_pairs={{0,4},{4,0},{1,5},{5,1},{2,6},{6,2},{3,7},{7,3},{8,12},{12,8},{9,1... | collective-permute-start | bytes 1081352 | tf_op jit(solution)/shard_map/ppermute | solution.py:116
  179.4 25.2 %collective-permute-start.40 = (bf16[704,256]{1,0:T(8,128)(2,1)S(1)}, bf16[704,256]{1,0:T(8,128)(2,1)S(1)}, u32[]{:S(2)}, u32[]{:S(2)}) collective-permute-start(bf16[704,256]{1,0:T(8,128)(2,1)S(1)} %collective-permute-done.33.refs_1_), channel_id=1, source_target_pairs={{0,4},{4,0},{1,5},{5,1},{2,6},{6,2},{3,7},{7,3},{8,12},{12,8},{9,1... | collective-permute-start | bytes 1081352 | tf_op jit(solution)/shard_map/ppermute | solution.py:116
  179.9 24.7 %collective-permute-start.41 = (bf16[704,256]{1,0:T(8,128)(2,1)S(1)}, bf16[704,256]{1,0:T(8,128)(2,1)S(1)}, u32[]{:S(2)}, u32[]{:S(2)}) collective-permute-start(bf16[704,256]{1,0:T(8,128)(2,1)S(1)} %collective-permute-done.34.refs_2_), channel_id=1, source_target_pairs={{0,4},{4,0},{1,5},{5,1},{2,6},{6,2},{3,7},{7,3},{8,12},{12,8},{9,1... | collective-permute-start | bytes 1081352 | tf_op jit(solution)/shard_map/ppermute | solution.py:116
  181.4 30.0 %collective-permute-start.42 = (bf16[704,256]{1,0:T(8,128)(2,1)S(1)}, bf16[704,256]{1,0:T(8,128)(2,1)S(1)}, u32[]{:S(2)}, u32[]{:S(2)}) collective-permute-start(bf16[704,256]{1,0:T(8,128)(2,1)S(1)} %collective-permute-done.35.refs_3_), channel_id=1, source_target_pairs={{0,4},{4,0},{1,5},{5,1},{2,6},{6,2},{3,7},{7,3},{8,12},{12,8},{9,1... | collective-permute-start | bytes 1081352 | tf_op jit(solution)/shard_map/ppermute | solution.py:116
  214.9 3.5 %collective-permute-start.43 = (bf16[1536,512]{1,0:T(8,128)(2,1)S(1)}, bf16[1536,512]{1,0:T(8,128)(2,1)S(1)}, u32[]{:S(2)}, u32[]{:S(2)}) collective-permute-start(bf16[1536,512]{1,0:T(8,128)(2,1)S(1)} %shard_map.125), channel_id=1, source_target_pairs={{0,1},{1,0},{2,3},{3,2},{4,5},{5,4},{6,7},{7,6},{8,9},{9,8},{10,11... | collective-permute-start | bytes 4718600 | tf_op jit(solution)/shard_map/ppermute | solution.py:116
  217.2 4.1 %collective-permute-start.36 = (bf16[1536,512]{1,0:T(8,128)(2,1)S(1)}, bf16[1536,512]{1,0:T(8,128)(2,1)S(1)}, u32[]{:S(2)}, u32[]{:S(2)}) collective-permute-start(bf16[1536,512]{1,0:T(8,128)(2,1)S(1)} %shard_map.123), channel_id=1, source_target_pairs={{0,1},{1,0},{2,3},{3,2},{4,5},{5,4},{6,7},{7,6},{8,9},{9,8},{10,11... | collective-permute-start | bytes 4718600 | tf_op jit(solution)/shard_map/ppermute | solution.py:116
  220.6 19.6 %collective-permute-start.44 = (bf16[1536,256]{1,0:T(8,128)(2,1)S(1)}, bf16[1536,256]{1,0:T(8,128)(2,1)S(1)}, u32[]{:S(2)}, u32[]{:S(2)}) collective-permute-start(bf16[1536,256]{1,0:T(8,128)(2,1)S(1)} %slice.47), channel_id=1, source_target_pairs={{0,2},{2,0},{1,3},{3,1},{4,6},{6,4},{5,7},{7,5},{8,10},{10,8},{9,1... | collective-permute-start | bytes 2359304 | tf_op jit(solution)/shard_map/ppermute | solution.py:116
  223.5 19.4 %collective-permute-start.37 = (bf16[768,512]{1,0:T(8,128)(2,1)S(1)}, bf16[768,512]{1,0:T(8,128)(2,1)S(1)}, u32[]{:S(2)}, u32[]{:S(2)}) collective-permute-start(bf16[768,512]{1,0:T(8,128)(2,1)S(1)} %slice.43), channel_id=1, source_target_pairs={{0,8},{8,0},{1,9},{9,1},{2,10},{10,2},{3,11},{11,3},{4,12},{12,4},... | collective-permute-start | bytes 2359304 | tf_op jit(solution)/shard_map/ppermute | solution.py:116
  241.3 10.3 %collective-permute-start.45 = (bf16[768,256]{1,0:T(8,128)(2,1)S(1)}, bf16[768,256]{1,0:T(8,128)(2,1)S(1)}, u32[]{:S(2)}, u32[]{:S(2)}) collective-permute-start(bf16[768,256]{1,0:T(8,128)(2,1)S(1)} %get-tuple-element.21), channel_id=1, source_target_pairs={{0,8},{8,0},{1,9},{9,1},{2,10},{10,2},{3,11},{11,3},{4,12},{12,4},... | collective-permute-start | bytes 1179656 | tf_op jit(solution)/shard_map/ppermute | solution.py:116
  244.0 10.1 %collective-permute-start.38 = (bf16[768,256]{1,0:T(8,128)(2,1)S(1)}, bf16[768,256]{1,0:T(8,128)(2,1)S(1)}, u32[]{:S(2)}, u32[]{:S(2)}) collective-permute-start(bf16[768,256]{1,0:T(8,128)(2,1)S(1)} %get-tuple-element.23), channel_id=1, source_target_pairs={{0,2},{2,0},{1,3},{3,1},{4,6},{6,4},{5,7},{7,5},{8,10},{10,8},{9,1... | collective-permute-start | bytes 1179656 | tf_op jit(solution)/shard_map/ppermute | solution.py:116
  (18 other events, 191.5 us)
